TPU v7x, 32 devices: a whole 2x2x4 slice. The times are simulated.
32 devices in a mesh: grp: 2 (over y), ep: 4 (over z), tp: 4 (over x, core).
Axes of the slice: x: 2, y: 2, z: 4, core: 2. Of those that a mesh axis runs over, the one named last changes fastest.
Arguments:
- outer_gate: bfloat16 [2048, 2048], P(('grp', 'ep'), 'tp'), parts along dimension 0, may hold values from -6 to 6
- inner_gate: bfloat16 [2048, 2048], P(('grp', 'ep'), 'tp'), parts along dimension 0, may hold values from -6 to 6
- inner_value: bfloat16 [2048, 2048], P(('grp', 'ep'), 'tp'), parts along dimension 0, may hold values from -6 to 6
- conv_taps: bfloat16 [3, 2048], replicated, may hold values from -3 to 3
- mixer_out: bfloat16 [2048, 2048], P('tp'), may hold values from -0.125 to 0.125
- mixer_gain: float32 [2048], replicated, may hold values from 0.1 to 1.9
- moe_tokens: bfloat16 [2048, 2048], P(('grp', 'ep', 'tp')), parts along dimension 0, may hold values from -6 to 6
- expert_gain: float32 [2048], replicated, may hold values from 0.1 to 1.9
- route_ids: int32 [2048, 4], P(('grp', 'ep', 'tp')), parts along dimension 0, may hold values from 0 to 15, all different within a row; in each aligned block of 64 rows (0 to 63, 64 to 127, ...) at most 24 rows name the same one
- route_weights: float32 [2048, 4], P(('grp', 'ep', 'tp')), parts along dimension 0, may hold values from 0.2 to 1
- expert_gate: bfloat16 [16, 2048, 512], P(('ep', 'tp')), may hold values from -0.125 to 0.125
- expert_up: bfloat16 [16, 2048, 512], P(('ep', 'tp')), may hold values from -0.125 to 0.125
- expert_down: bfloat16 [16, 512, 2048], P(('ep', 'tp')), may hold values from -0.25 to 0.25
- shared_gate: bfloat16 [2048, 512], P(None, 'tp'), may hold values from -0.125 to 0.125
- shared_up: bfloat16 [2048, 512], P(None, 'tp'), may hold values from -0.125 to 0.125
- shared_down: bfloat16 [512, 2048], P('tp'), may hold values from -0.25 to 0.25
Outputs:
- mixed_rows: bfloat16 [2048, 2048], P(('grp', 'ep', 'tp')), parts along dimension 0
- expert_rows: bfloat16 [2048, 2048], P(('grp', 'ep', 'tp')), parts along dimension 0
There are 2 independent parts, one for each index of `grp`. A program takes and returns all parts, laid end to end along the dimension named above; an argument that names none is the same for every part. Nothing has to cross between parts.
Inputs may be any that keep to these rules, and one draw needn't show every extreme that they name: `route_ids`: each row names 4 different experts; among the 64 rows of one device (aligned blocks) no expert is named more than 24 times, a bound that some block reaches.
All inputs are finite; a program needn't handle non-finite values.
Results may differ from a plain program's by a relative error of at most 0.012.
Values may be sent and summed in bfloat16 or wider, within the bound.
A program may use at most 64 MiB of HBM per device.

v0:
```python
import functools
import jax
import jax.numpy as jnp
from jax import lax
from jax.experimental import pallas as pl
from jax.experimental.pallas import tpu as pltpu
from jax.sharding import PartitionSpec as P

EPSILON = 1e-06


def passed_along(array, axis, by):
    size = lax.axis_size(axis)
    pairs = [(i, i + by) for i in range(size) if 0 <= i + by < size]
    return lax.ppermute(array, axis, pairs)


def rms_scale(values, gains):
    return values * lax.rsqrt(jnp.mean(values * values, axis=-1, keepdims=True) + EPSILON) * gains


def on_device(
    outer_gate,
    inner_gate,
    inner_value,
    conv_taps,
    mixer_out,
    mixer_gain,
    moe_tokens,
    expert_gain,
    route_ids,
    route_weights,
    expert_gate,
    expert_up,
    expert_down,
    shared_gate,
    shared_up,
    shared_down,
):
    columns = inner_gate.shape[1]
    kernel = lax.dynamic_slice_in_dim(conv_taps, lax.axis_index("tp") * columns, columns, 1).astype(
        jnp.float32
    )
    before_gate, before_value = passed_along((inner_gate[-2:], inner_value[-2:]), "ep", 1)
    gate_rows = jnp.concatenate([before_gate, inner_gate], axis=0).astype(jnp.float32)
    value_rows = jnp.concatenate([before_value, inner_value], axis=0).astype(jnp.float32)
    product = gate_rows * value_rows
    filtered = kernel[0] * product[:-2] + kernel[1] * product[1:-1] + kernel[2] * product[2:]
    scaled = (outer_gate.astype(jnp.float32) * filtered).astype(jnp.bfloat16)
    normed = rms_scale(moe_tokens.astype(jnp.float32), expert_gain).astype(jnp.bfloat16)
    feature_width = normed.shape[1]
    piece = lax.all_gather(normed, "tp", axis=0, tiled=True)
    gate_value = jnp.dot(piece, shared_gate, preferred_element_type=jnp.float32)
    up_value = jnp.dot(piece, shared_up, preferred_element_type=jnp.float32)
    shared_act = (jax.nn.silu(gate_value) * up_value).astype(jnp.bfloat16)
    mixer_part = jnp.dot(scaled, mixer_out, preferred_element_type=jnp.float32)
    shared_part = jnp.dot(shared_act, shared_down, preferred_element_type=jnp.float32)
    both_sums = lax.psum_scatter(
        jnp.concatenate([mixer_part, shared_part], axis=1).astype(jnp.bfloat16),
        "tp",
        scatter_dimension=0,
        tiled=True,
    ).astype(jnp.float32)
    mixed_rows = rms_scale(both_sums[:, :feature_width], mixer_gain).astype(jnp.bfloat16)
    shared_out = both_sums[:, feature_width:]
    row_count, top_count = route_ids.shape
    ep_count = lax.axis_size("ep")
    tp_count = lax.axis_size("tp")
    expert_count = ep_count * tp_count
    capacity = (3 * row_count * top_count + 2 * expert_count - 1) // (2 * expert_count)
    flat_ids = route_ids.reshape(-1)
    onehot = (flat_ids[:, None] == jnp.arange(expert_count, dtype=jnp.int32)[None, :]).astype(
        jnp.int32
    )
    slot_rank = jnp.sum(
        (jnp.cumsum(onehot, axis=0, dtype=jnp.int32) - onehot) * onehot, axis=1, dtype=jnp.int32
    )
    target = flat_ids * capacity + slot_rank
    token_of = jnp.arange(flat_ids.shape[0], dtype=jnp.int32) // top_count
    slot_token = jnp.zeros((expert_count * capacity,), jnp.int32).at[target].set(token_of)
    outgoing = normed[slot_token].reshape(expert_count, capacity, feature_width)
    arrived = lax.all_to_all(outgoing, ("ep", "tp"), split_axis=0, concat_axis=0, tiled=True)
    flat_in = arrived.reshape(expert_count * capacity, feature_width)
    gate_value = jnp.dot(flat_in, expert_gate[0], preferred_element_type=jnp.float32)
    up_value = jnp.dot(flat_in, expert_up[0], preferred_element_type=jnp.float32)
    active = (jax.nn.silu(gate_value) * up_value).astype(jnp.bfloat16)
    result = jnp.dot(active, expert_down[0], preferred_element_type=jnp.float32).astype(
        jnp.bfloat16
    )
    returned = lax.all_to_all(
        result.reshape(expert_count, capacity, feature_width),
        ("ep", "tp"),
        split_axis=0,
        concat_axis=0,
        tiled=True,
    )
    picked = returned.reshape(expert_count * capacity, feature_width)[target].astype(jnp.float32)
    weights = route_weights.reshape(-1)
    routed = jnp.sum(
        (weights[:, None] * picked).reshape(row_count, top_count, feature_width), axis=1
    )
    expert_rows = (shared_out + routed).astype(jnp.bfloat16)
    return (mixed_rows, expert_rows)


MESH = pl.DeviceIdType.MESH
BF = jnp.bfloat16
F32 = jnp.float32
CHUNKS = 2
PARTS = 2
PIECES = (CHUNKS,) + tuple(range(CHUNKS))


def dot(a, b):
    return jnp.dot(a, b, preferred_element_type=F32)


def fused_kernel(
    ep, tp, cap,
    og_h, ig_h, iv_h, taps, mo_h, mgain, tok_h, egain, ids, wts, eg_h, eu_h, ed_h, sg_h, su_h, sd_h,
    mixed_ref, rows_ref,
    og, ig, iv, mo, tok, eg, eu, ed, sgu, sd, halo, pbuf, scaled,
    gat, tab, xs, act, ys, sact, dd, rc, rx, zd, zu, mp, mrc, mrx,
    load_sem, halo_sem, gz_r, gz_su, gz_sd, gx_r, gx_s, gc_r, gc_s,
    rc_r, rc_s, rx_r, rx_s, zd_r, zd_s, zu_r, zu_s, m_r, m_s,
):
    z = lax.axis_index("ep")
    t = lax.axis_index("tp")
    g = lax.axis_index("grp")
    x = t // 2
    c = t % 2
    rows = tok.shape[0]
    width = tok.shape[1]
    columns = ig.shape[1]
    sub = rows // CHUNKS
    up = (g, z + 1, t)
    down = (g, z - 1, t)
    xn = (g, z, (1 - x) * 2 + c)
    pc = (g, z, x * 2 + 1 - c)
    has_up = z < ep - 1
    has_down = z > 0

    loads = {}

    def load(name, src, dst):
        copy = pltpu.make_async_copy(src, dst, load_sem.at[len(loads)])
        copy.start()
        loads[name] = copy

    half = sd.shape[0]
    load("tok", tok_h, tok)
    load("ig", ig_h, ig)
    load("iv", iv_h, iv)
    load("og", og_h, og)
    load("mo", mo_h, mo)
    load("sg", sg_h, sgu.at[:, pl.ds(0, half)])
    load("su", su_h, sgu.at[:, pl.ds(half, half)])
    load("sd", sd_h, sd)
    load("eg", eg_h.at[0], eg)
    load("eu", eu_h.at[0], eu)
    load("ed", ed_h.at[0], ed)

    barrier = pltpu.get_barrier_semaphore()
    for peer in (xn, pc):
        pl.semaphore_signal(barrier, inc=1, device_id=peer, device_id_type=MESH)

    @pl.when(has_up)
    def _():
        pl.semaphore_signal(barrier, inc=1, device_id=up, device_id_type=MESH)

    @pl.when(has_down)
    def _():
        pl.semaphore_signal(barrier, inc=1, device_id=down, device_id_type=MESH)

    def rcopy(src, dst, ssem, rsem, peer):
        return pltpu.make_async_remote_copy(
            src_ref=src, dst_ref=dst, send_sem=ssem, recv_sem=rsem, device_id=peer, device_id_type=MESH
        )

    def block(zz, xx, cc):
        return (zz * 2 + xx) * 2 + cc

    def piece(zz, xx, cc, k):
        if k == CHUNKS:
            return tab.at[block(zz, xx, cc)]
        return gat.at[pl.ds(pl.multiple_of(block(zz, xx, cc) * rows + k * sub, sub), sub), :]

    def whole(zz, xx, cc):
        return gat.at[pl.ds(pl.multiple_of(block(zz, xx, cc) * rows, rows), rows), :]

    def c_up(zz, k):
        return rcopy(piece(zz, x, c, k), piece(zz, x, c, k), gz_su.at[zz, k], gz_r.at[zz, k], up)

    def c_down(zz, k):
        return rcopy(piece(zz, x, c, k), piece(zz, x, c, k), gz_sd.at[zz, k], gz_r.at[zz, k], down)

    def c_x(zz, k):
        return rcopy(piece(zz, x, c, k), piece(zz, x, c, k), gx_s.at[zz, k], gx_r.at[zz, k], xn)

    def x_arrival(zz, k):
        return rcopy(piece(zz, 1 - x, c, k), piece(zz, 1 - x, c, k), gx_s.at[zz, k], gx_r.at[zz, k], xn)

    def core_pair(zz, xx, cc):
        names = tab.at[block(zz, xx, cc)]
        return (
            rcopy(whole(zz, xx, cc), whole(zz, xx, cc), gc_s.at[zz, xx, 0], gc_r.at[zz, xx, 0], pc),
            rcopy(names, names, gc_s.at[zz, xx, 1], gc_r.at[zz, xx, 1], pc),
        )

    def core_start(zz, xx):
        for copy in core_pair(zz, xx, c):
            copy.start()

    loads["tok"].wait()
    name_i = lax.broadcasted_iota(jnp.int32, (tab.shape[1], rows), 0)
    table = jnp.zeros((tab.shape[1], rows), F32)
    for k in range(ids.shape[0]):
        table = table + jnp.where(ids[k : k + 1, :] == name_i, wts[k : k + 1, :], 0.0)
    tab[block(z, x, c)] = jnp.zeros(tab.shape[1:], BF)
    tab[block(z, x, c), :, :rows] = table.astype(BF)
    v = tok[...].astype(F32)
    v = v * lax.rsqrt(jnp.mean(v * v, axis=-1, keepdims=True) + EPSILON) * egain[...]
    own = pl.ds(pl.multiple_of(block(z, x, c) * rows, rows), rows)
    gat[own, :] = v.astype(BF)

    pl.semaphore_wait(barrier, 2 + jnp.minimum(z, 1) + jnp.minimum(ep - 1 - z, 1))

    for k in PIECES:
        @pl.when(has_up)
        def _():
            c_up(z, k).start()

        @pl.when(has_down)
        def _():
            c_down(z, k).start()

        c_x(z, k).start()
    core_start(z, x)

    loads["ig"].wait()
    loads["iv"].wait()
    tail = ig.shape[0] - halo.shape[1]
    edge = halo.shape[1]
    h_gate = rcopy(ig.at[pl.ds(tail, edge)], halo.at[0], halo_sem.at[0], halo_sem.at[1], up)
    h_value = rcopy(iv.at[pl.ds(tail, edge)], halo.at[1], halo_sem.at[2], halo_sem.at[3], up)

    @pl.when(has_up)
    def _():
        h_gate.start()
        h_value.start()

    count = ig.shape[0]
    pbuf[8:, :] = ig[...].astype(F32) * iv[...].astype(F32)

    @pl.when(jnp.logical_not(has_down))
    def _():
        pbuf[:8, :] = jnp.zeros((8, columns), F32)

    @pl.when(has_down)
    def _():
        h_gate.wait_recv()
        h_value.wait_recv()
        pbuf[:8, :] = halo[0, edge - 8 :, :].astype(F32) * halo[1, edge - 8 :, :].astype(F32)

    loads["og"].wait()
    tap = taps[:, pl.ds(pl.multiple_of(t * columns, columns), columns)].astype(F32)
    filtered = (
        tap[0:1] * pbuf[6 : 6 + count, :] + tap[1:2] * pbuf[7 : 7 + count, :] + tap[2:3] * pbuf[8 : 8 + count, :]
    )
    scaled[...] = (og[...].astype(F32) * filtered).astype(BF)
    loads["mo"].wait()
    tile = width // 4

    def cols(n):
        return pl.ds(pl.multiple_of(n * tile, tile), tile)

    @pl.loop(0, 4)
    def _(n):
        part = dot(scaled[...], mo[:, cols(n)]).astype(BF)
        mp[:, :, cols(n)] = part.reshape(tp, rows, tile)

    def m_core(xx):
        return rcopy(mp.at[xx * 2 + 1 - c], mrc.at[xx], m_s.at[xx], m_r.at[xx], pc)

    for xx in range(2):
        m_core(xx).start()

    def z_step(s):
        for k in PIECES:
            @pl.when(z >= s)
            def _():
                c_up(z - s, k).wait_recv()

                @pl.when(has_up)
                def _():
                    c_up(z - s, k).start()

                c_x(z - s, k).start()

            @pl.when(z + s < ep)
            def _():
                c_down(z + s, k).wait_recv()

                @pl.when(has_down)
                def _():
                    c_down(z + s, k).start()

                c_x(z + s, k).start()

        @pl.when(z >= s)
        def _():
            core_start(z - s, x)

        @pl.when(z + s < ep)
        def _():
            core_start(z + s, x)

    def x_step(zz):
        for k in PIECES:
            x_arrival(zz, k).wait_recv()
        core_start(zz, 1 - x)

    def core_step(zz):
        for xx in range(2):
            for copy in core_pair(zz, xx, 1 - c):
                copy.wait_recv()

    def nth(n):
        near = jnp.minimum(z, ep - 1 - z)
        d = (n + 1) // 2
        side = z - d if n % 2 else z + d
        far = jnp.where(z < ep - 1 - z, n, ep - 1 - n)
        return jnp.where(n <= 2 * near, side, far)

    order = [nth(n) for n in range(ep)]

    def group(zz):
        return pl.ds(pl.multiple_of(zz * tp * rows, tp * rows), tp * rows)

    tokens = tp * rows
    slots = tp * cap
    expert = z * tp + t
    picked = lax.broadcasted_iota(jnp.int32, (tab.shape[1], tab.shape[2]), 0) == expert
    ti = lax.broadcasted_iota(jnp.int32, (tokens, tokens), 0)
    tj = lax.broadcasted_iota(jnp.int32, (tokens, tokens), 1)
    before = jnp.logical_and(ti < tj, ti // rows == tj // rows).astype(BF)
    slot_i = lax.broadcasted_iota(jnp.int32, (slots, tokens), 0)
    base = (lax.broadcasted_iota(jnp.int32, (1, tokens), 1) // rows) * cap

    def select(zz):
        lines = [
            jnp.sum(jnp.where(picked, tab[zz * tp + i].astype(F32), 0.0), axis=0, keepdims=True)[:, :rows]
            for i in range(tp)
        ]
        weight = jnp.broadcast_to(jnp.concatenate(lines, axis=1), (8, tokens))
        named = weight > 0
        rank = dot(named.astype(F32).astype(BF), before)[0:1].astype(jnp.int32) + base
        hit = jnp.logical_and(slot_i == rank, named[0:1])
        return hit.astype(F32).astype(BF), jnp.where(hit, weight[0:1], 0.0).astype(BF)

    def experts(pair):
        marks = [select(zz) for zz in pair]
        for i, zz in enumerate(pair):
            spot = pl.ds(i * slots, slots)

            @pl.loop(0, 4)
            def _(n):
                xs[spot, cols(n)] = dot(marks[i][0], gat[group(zz), cols(n)]).astype(BF)

        hid = act.shape[1] // 2

        @pl.loop(0, 2)
        def _(n):
            col = pl.ds(pl.multiple_of(n * hid, hid), hid)
            gate = dot(xs[...], eg[:, col])
            value = dot(xs[...], eu[:, col])
            act[:, col] = (gate / (1.0 + jnp.exp(-gate)) * value).astype(BF)

        @pl.loop(0, 4)
        def _(n):
            ys[:, cols(n)] = dot(act[...], ed[:, cols(n)]).astype(BF)

        for i, zz in enumerate(pair):
            is_own = zz == z

            @pl.loop(0, 4)
            def _(n):
                out = lax.dot_general(
                    marks[i][1],
                    ys[pl.ds(i * slots, slots), cols(n)],
                    (((0,), (0,)), ((), ())),
                    preferred_element_type=F32,
                )
                dst = pl.ds(pl.multiple_of(zz * tp, tp), tp)
                if zz is order[0]:
                    out = out + dot(sact[...], sd[:, cols(n)])
                dd[dst, :, cols(n)] = out.astype(BF).reshape(tp, rows, tile)

    def d_core(zz, xx):
        return rcopy(dd.at[block(zz, xx, 1 - c)], rc.at[zz, xx], rc_s.at[zz, xx], rc_r.at[zz, xx], pc)

    deep = rows // PARTS

    def part_of(ref, p):
        return ref.at[pl.ds(p * deep, deep)]

    def d_x(zz, p):
        src = part_of(dd.at[block(zz, 1 - x, c)], p)
        return rcopy(src, part_of(rx.at[zz], p), rx_s.at[zz, p], rx_r.at[zz, p], xn)

    def d_up(zz, p):
        src = part_of(dd.at[block(zz, x, c)], p)
        return rcopy(src, part_of(zu.at[zz], p), zu_s.at[zz, p], zu_r.at[zz, p], up)

    def d_down(zz, p):
        src = part_of(dd.at[block(zz, x, c)], p)
        return rcopy(src, part_of(zd.at[zz], p), zd_s.at[zz, p], zd_r.at[zz, p], down)

    z_step(1)

    x_step(order[0])
    z_step(2)
    core_step(order[0])
    for name in ("sg", "su", "sd"):
        loads[name].wait()
    hidden = dot(gat[group(z), :], sgu[...])
    gate, value = hidden[:, :half], hidden[:, half:]
    sact[...] = (gate / (1.0 + jnp.exp(-gate)) * value).astype(BF)
    for s in range(3, ep):
        z_step(s)

    m_x = rcopy(mp.at[(1 - x) * 2 + c], mrx, m_s.at[2], m_r.at[2], xn)
    for xx in range(2):
        m_core(xx).wait_recv()
    mine = (1 - x) * 2 + c
    mp[mine] = (mp[mine].astype(F32) + mrc[1 - x].astype(F32)).astype(BF)
    m_x.start()

    x_step(order[1])
    core_step(order[1])
    for name in ("eg", "eu", "ed"):
        loads[name].wait()
    for n in range(0, ep, 2):
        pair = order[n : n + 2]
        if n:
            for zz in pair:
                x_step(zz)
            for zz in pair:
                core_step(zz)
        experts(pair)
        for zz in pair[::-1]:
            for xx in range(2):
                d_core(zz, xx).start()

    for zz in order[::-1]:
        for xx in range(2):
            d_core(zz, xx).wait_recv()
        there = block(zz, 1 - x, c)
        dd[there] = (dd[there].astype(F32) + rc[zz, 1 - x].astype(F32)).astype(BF)
        for p in range(PARTS):
            d_x(zz, p).start()

    m_x.wait_recv()
    mixed = mp[t].astype(F32) + mrc[x].astype(F32) + mrx[...].astype(F32)
    scale = lax.rsqrt(jnp.mean(mixed * mixed, axis=-1, keepdims=True) + EPSILON)
    mixed_ref[...] = (mixed * scale * mgain[...]).astype(BF)

    for zz in order[:0:-1]:
        here = block(zz, x, c)
        lower = zz < z
        for p in range(PARTS):
            band = pl.ds(p * deep, deep)
            d_x(zz, p).wait_recv()
            so_far = (
                dd[here, band].astype(F32) + rc[zz, x, band].astype(F32) + rx[zz, band].astype(F32)
            )

            @pl.when(jnp.logical_and(lower, has_up))
            def _():
                d_down(zz, p).wait_recv()
                dd[here, band] = (so_far + zd[zz, band].astype(F32)).astype(BF)

            @pl.when(jnp.logical_and(jnp.logical_not(lower), has_down))
            def _():
                d_up(zz, p).wait_recv()
                dd[here, band] = (so_far + zu[zz, band].astype(F32)).astype(BF)

            @pl.when(jnp.where(lower, jnp.logical_not(has_up), jnp.logical_not(has_down)))
            def _():
                dd[here, band] = so_far.astype(BF)

            @pl.when(lower)
            def _():
                d_down(zz, p).start()

            @pl.when(jnp.logical_not(lower))
            def _():
                d_up(zz, p).start()

    here = block(z, x, c)
    for p in range(PARTS):
        band = pl.ds(p * deep, deep)
        d_x(z, p).wait_recv()
        total = dd[here, band].astype(F32) + rc[z, x, band].astype(F32) + rx[z, band].astype(F32)

        @pl.when(jnp.logical_not(has_up))
        def _():
            d_up(z, p).wait_recv()
            rows_ref[band, :] = (total + zu[z, band].astype(F32)).astype(BF)

        @pl.when(jnp.logical_not(has_down))
        def _():
            d_down(z, p).wait_recv()
            rows_ref[band, :] = (total + zd[z, band].astype(F32)).astype(BF)

        @pl.when(jnp.logical_and(has_up, has_down))
        def _():
            d_up(z, p).wait_recv()
            d_down(z, p).wait_recv()
            rows_ref[band, :] = (
                total + zu[z, band].astype(F32) + zd[z, band].astype(F32)
            ).astype(BF)

    @pl.when(has_up)
    def _():
        h_gate.wait_send()
        h_value.wait_send()

    for zz in range(ep):
        @pl.when(jnp.logical_and(has_up, zz <= z))
        def _():
            for k in PIECES:
                c_up(zz, k).wait_send()

        @pl.when(jnp.logical_and(has_down, zz >= z))
        def _():
            for k in PIECES:
                c_down(zz, k).wait_send()

        for k in PIECES:
            c_x(zz, k).wait_send()
        for xx in range(2):
            for copy in core_pair(zz, xx, c):
                copy.wait_send()
            d_core(zz, xx).wait_send()
        for p in range(PARTS):
            d_x(zz, p).wait_send()

        @pl.when(zz < z)
        def _():
            for p in range(PARTS):
                d_down(zz, p).wait_send()

        @pl.when(zz > z)
        def _():
            for p in range(PARTS):
                d_up(zz, p).wait_send()

    for xx in range(2):
        m_core(xx).wait_send()
    m_x.wait_send()


def fused_on_device(ep, tp, *args):
    (og, ig, iv, taps, mo, mgain, tok, egain, ids, wts, eg, eu, ed, sg, su, sd) = args
    rows, width = tok.shape
    count, columns = ig.shape
    experts = ep * tp
    cap = (3 * rows * ids.shape[1] + 2 * experts - 1) // (2 * experts)
    names = -(-experts // 16) * 16
    hid = eg.shape[2]
    half = sd.shape[0]
    any_spec = pl.BlockSpec(memory_space=pl.ANY)
    vmem = pl.BlockSpec(memory_space=pltpu.VMEM)
    dma = pltpu.SemaphoreType.DMA
    V = pltpu.VMEM
    return pl.pallas_call(
        functools.partial(fused_kernel, ep, tp, cap),
        out_shape=(jax.ShapeDtypeStruct((rows, width), BF), jax.ShapeDtypeStruct((rows, width), BF)),
        in_specs=[any_spec] * 3 + [vmem, any_spec, vmem, any_spec, vmem, vmem, vmem] + [any_spec] * 6,
        out_specs=(vmem, vmem),
        scratch_shapes=[
            V((count, columns), BF), V((count, columns), BF), V((count, columns), BF),
            V((columns, width), BF), V((rows, width), BF),
            V((width, hid), BF), V((width, hid), BF), V((hid, width), BF),
            V((width, 2 * half), BF), V((half, width), BF),
            V((2, 16, columns), BF), V((count + 8, columns), F32), V((count, columns), BF),
            V((experts * rows, width), BF), V((experts, names, 128), BF),
            V((2 * tp * cap, width), BF), V((2 * tp * cap, hid), BF), V((2 * tp * cap, width), BF),
            V((tp * rows, half), BF),
            V((experts, rows, width), BF), V((ep, 2, rows, width), BF), V((ep, rows, width), BF),
            V((ep, rows, width), BF), V((ep, rows, width), BF),
            V((tp, rows, width), BF), V((2, rows, width), BF), V((rows, width), BF),
            dma((11,)), dma((4,)),
            dma((ep, CHUNKS + 1)), dma((ep, CHUNKS + 1)), dma((ep, CHUNKS + 1)),
            dma((ep, CHUNKS + 1)), dma((ep, CHUNKS + 1)), dma((ep, 2, 2)), dma((ep, 2, 2)),
            dma((ep, 2)), dma((ep, 2)), dma((ep, PARTS)), dma((ep, PARTS)),
            dma((ep, PARTS)), dma((ep, PARTS)), dma((ep, PARTS)), dma((ep, PARTS)), dma((3,)), dma((3,)),
        ],
        compiler_params=pltpu.CompilerParams(
            collective_id=0, has_side_effects=True, vmem_limit_bytes=60 * 1024 * 1024
        ),
    )(
        og, ig, iv, taps, mo, mgain.reshape(1, -1), tok, egain.reshape(1, -1), ids.T, wts.T, eg, eu, ed, sg, su, sd
    )


def plan(mesh):
    ep, tp = mesh.shape["ep"], mesh.shape["tp"]
    if tp == 4 and ep % 2 == 0 and ep <= 4:
        return functools.partial(fused_on_device, ep, tp)
    return on_device


def solution(mesh):
    return jax.shard_map(
        plan(mesh),
        mesh=mesh,
        in_specs=(
            P(("grp", "ep"), "tp"),
            P(("grp", "ep"), "tp"),
            P(("grp", "ep"), "tp"),
            P(),
            P("tp", None),
            P(),
            P(("grp", "ep", "tp"), None),
            P(),
            P(("grp", "ep", "tp"), None),
            P(("grp", "ep", "tp"), None),
            P(("ep", "tp"), None, None),
            P(("ep", "tp"), None, None),
            P(("ep", "tp"), None, None),
            P(None, "tp"),
            P(None, "tp"),
            P("tp", None),
        ),
        out_specs=(P(("grp", "ep", "tp"), None), P(("grp", "ep", "tp"), None)),
        check_vma=False,
    )
```

profile of v0, /device:TPU:0, one launch (start us, length us, event | category | flops | bytes accessed | tf_op | source)
XLA Modules:
  0.0 73.8 jit_solution(6438368074301424455)
XLA Ops:
  0.6 69.8 %shard_map.167 = (bf16[64,2048]{1,0:T(8,128)(2,1)}, bf16[64,2048]{1,0:T(8,128)(2,1)}) custom-call(bf16[256,512]{1,0:T(8,128)(2,1)} %og_h.1, bf16[256,512]{1,0:T(8,128)(2,1)} %ig_h.1, bf16[256,512]{1,0:T(8,128)(2,1)} %iv_h.1, bf16[3,2048]{1,0:T(4,128)(2,1)} %taps.1, bf16[512,2048]{1,0:T(8,128)(2,1)} %mo_h.1, f32[1,2048]{1,0:T(1,128)} %bitcast.4, ...), custom_call_target="tpu_custom_call" | custom-call | tf_op jit(solution)/shard_map/pallas_call | solution.py:577
  70.4 1.7 %copy.20 = bf16[64,2048]{1,0:T(8,128)(2,1)} copy(bf16[64,2048]{1,0:T(8,128)(2,1)} %get-tuple-element.4) | data formatting | bytes 524288
  72.1 1.7 %copy.21 = bf16[64,2048]{1,0:T(8,128)(2,1)} copy(bf16[64,2048]{1,0:T(8,128)(2,1)} %get-tuple-element.5) | data formatting | bytes 524288
where the time goes:
time: 74.5 us; the launch traced here: 73.8 us
  Pallas kernels  69.8 us (94%)
  local copies, waits for them, and re-layouts  3.34 us (4%)
    pallas_call x1, Pallas kernels, fused_on_device(): pl.pallas_call(functools.partial(fused_kernel, ep, tp, cap), out_shape=(j...  69.8 us
    unnamed x2, local copies, waits for them, and re-layouts  3.34 us

commit v1 on v0

--- a/solution.py
+++ b/solution.py
@@ -107,7 +107,7 @@
 BF = jnp.bfloat16
 F32 = jnp.float32
 CHUNKS = 2
-PARTS = 2
+PARTS = 4
 PIECES = (CHUNKS,) + tuple(range(CHUNKS))
 
 
@@ -116,11 +116,11 @@
 
 
 def fused_kernel(
-    ep, tp, cap,
+    ep, tp,
     og_h, ig_h, iv_h, taps, mo_h, mgain, tok_h, egain, ids, wts, eg_h, eu_h, ed_h, sg_h, su_h, sd_h,
     mixed_ref, rows_ref,
-    og, ig, iv, mo, tok, eg, eu, ed, sgu, sd, halo, pbuf, scaled,
-    gat, tab, xs, act, ys, sact, dd, rc, rx, zd, zu, mp, mrc, mrx,
+    og, ig, iv, mo, tok, eg, eu, ed, sgu, halo, pbuf, scaled,
+    gat, tab, act, dd, rc, rx, zd, zu, mp, mrc, mrx,
     load_sem, halo_sem, gz_r, gz_su, gz_sd, gx_r, gx_s, gc_r, gc_s,
     rc_r, rc_s, rx_r, rx_s, zd_r, zd_s, zu_r, zu_s, m_r, m_s,
 ):
@@ -147,7 +147,8 @@
         copy.start()
         loads[name] = copy
 
-    half = sd.shape[0]
+    half = sd_h.shape[0]
+    hid = eg.shape[1]
     load("tok", tok_h, tok)
     load("ig", ig_h, ig)
     load("iv", iv_h, iv)
@@ -155,10 +156,10 @@
     load("mo", mo_h, mo)
     load("sg", sg_h, sgu.at[:, pl.ds(0, half)])
     load("su", su_h, sgu.at[:, pl.ds(half, half)])
-    load("sd", sd_h, sd)
+    load("sd", sd_h, ed.at[pl.ds(hid, half), :])
     load("eg", eg_h.at[0], eg)
     load("eu", eu_h.at[0], eu)
-    load("ed", ed_h.at[0], ed)
+    load("ed", ed_h.at[0], ed.at[pl.ds(0, hid), :])
 
     barrier = pltpu.get_barrier_semaphore()
     for peer in (xn, pc):
@@ -250,40 +251,41 @@
         h_value.start()
 
     count = ig.shape[0]
-    pbuf[8:, :] = ig[...].astype(F32) * iv[...].astype(F32)
-
-    @pl.when(jnp.logical_not(has_down))
-    def _():
-        pbuf[:8, :] = jnp.zeros((8, columns), F32)
-
-    @pl.when(has_down)
-    def _():
-        h_gate.wait_recv()
-        h_value.wait_recv()
-        pbuf[:8, :] = halo[0, edge - 8 :, :].astype(F32) * halo[1, edge - 8 :, :].astype(F32)
-
-    loads["og"].wait()
-    tap = taps[:, pl.ds(pl.multiple_of(t * columns, columns), columns)].astype(F32)
-    filtered = (
-        tap[0:1] * pbuf[6 : 6 + count, :] + tap[1:2] * pbuf[7 : 7 + count, :] + tap[2:3] * pbuf[8 : 8 + count, :]
-    )
-    scaled[...] = (og[...].astype(F32) * filtered).astype(BF)
-    loads["mo"].wait()
     tile = width // 4
 
     def cols(n):
         return pl.ds(pl.multiple_of(n * tile, tile), tile)
 
-    @pl.loop(0, 4)
-    def _(n):
-        part = dot(scaled[...], mo[:, cols(n)]).astype(BF)
-        mp[:, :, cols(n)] = part.reshape(tp, rows, tile)
-
     def m_core(xx):
         return rcopy(mp.at[xx * 2 + 1 - c], mrc.at[xx], m_s.at[xx], m_r.at[xx], pc)
 
-    for xx in range(2):
-        m_core(xx).start()
+    def mixer():
+        pbuf[8:, :] = ig[...].astype(F32) * iv[...].astype(F32)
+
+        @pl.when(jnp.logical_not(has_down))
+        def _():
+            pbuf[:8, :] = jnp.zeros((8, columns), F32)
+
+        @pl.when(has_down)
+        def _():
+            h_gate.wait_recv()
+            h_value.wait_recv()
+            pbuf[:8, :] = halo[0, edge - 8 :, :].astype(F32) * halo[1, edge - 8 :, :].astype(F32)
+
+        loads["og"].wait()
+        tap = taps[:, pl.ds(pl.multiple_of(t * columns, columns), columns)].astype(F32)
+        filtered = (
+            tap[0:1] * pbuf[6 : 6 + count, :] + tap[1:2] * pbuf[7 : 7 + count, :] + tap[2:3] * pbuf[8 : 8 + count, :]
+        )
+        scaled[...] = (og[...].astype(F32) * filtered).astype(BF)
+        loads["mo"].wait()
+        @pl.loop(0, 4)
+        def _(n):
+            part = dot(scaled[...], mo[:, cols(n)]).astype(BF)
+            mp[:, :, cols(n)] = part.reshape(tp, rows, tile)
+
+        for xx in range(2):
+            m_core(xx).start()
 
     def z_step(s):
         for k in PIECES:
@@ -338,63 +340,39 @@
         return pl.ds(pl.multiple_of(zz * tp * rows, tp * rows), tp * rows)
 
     tokens = tp * rows
-    slots = tp * cap
     expert = z * tp + t
     picked = lax.broadcasted_iota(jnp.int32, (tab.shape[1], tab.shape[2]), 0) == expert
-    ti = lax.broadcasted_iota(jnp.int32, (tokens, tokens), 0)
-    tj = lax.broadcasted_iota(jnp.int32, (tokens, tokens), 1)
-    before = jnp.logical_and(ti < tj, ti // rows == tj // rows).astype(BF)
-    slot_i = lax.broadcasted_iota(jnp.int32, (slots, tokens), 0)
-    base = (lax.broadcasted_iota(jnp.int32, (1, tokens), 1) // rows) * cap
-
-    def select(zz):
-        lines = [
-            jnp.sum(jnp.where(picked, tab[zz * tp + i].astype(F32), 0.0), axis=0, keepdims=True)[:, :rows]
-            for i in range(tp)
-        ]
-        weight = jnp.broadcast_to(jnp.concatenate(lines, axis=1), (8, tokens))
-        named = weight > 0
-        rank = dot(named.astype(F32).astype(BF), before)[0:1].astype(jnp.int32) + base
-        hit = jnp.logical_and(slot_i == rank, named[0:1])
-        return hit.astype(F32).astype(BF), jnp.where(hit, weight[0:1], 0.0).astype(BF)
-
-    def experts(pair):
-        marks = [select(zz) for zz in pair]
-        for i, zz in enumerate(pair):
-            spot = pl.ds(i * slots, slots)
-
-            @pl.loop(0, 4)
-            def _(n):
-                xs[spot, cols(n)] = dot(marks[i][0], gat[group(zz), cols(n)]).astype(BF)
-
-        hid = act.shape[1] // 2
-
-        @pl.loop(0, 2)
+    diagonal = lax.broadcasted_iota(jnp.int32, (rows, tab.shape[2]), 0) == lax.broadcasted_iota(
+        jnp.int32, (rows, tab.shape[2]), 1
+    )
+
+    def weight_column(block_id):
+        line = jnp.sum(jnp.where(picked, tab[block_id].astype(F32), 0.0), axis=0, keepdims=True)
+        return jnp.sum(jnp.where(diagonal, line, 0.0), axis=1, keepdims=True)
+
+    def shared():
+        for name in ("sg", "su", "sd"):
+            loads[name].wait()
+        hidden = dot(gat[group(z), :], sgu[...])
+        gate, value = hidden[:, :half], hidden[:, half:]
+        act[:, hid:] = (gate / (1.0 + jnp.exp(-gate)) * value).astype(BF)
+
+    def experts(zz, depth):
+        weight = jnp.concatenate([weight_column(zz * tp + i) for i in range(tp)], axis=0)
+        step = 256 if hid % 256 == 0 else hid
+
+        @pl.loop(0, hid // step)
         def _(n):
-            col = pl.ds(pl.multiple_of(n * hid, hid), hid)
-            gate = dot(xs[...], eg[:, col])
-            value = dot(xs[...], eu[:, col])
-            act[:, col] = (gate / (1.0 + jnp.exp(-gate)) * value).astype(BF)
+            col = pl.ds(pl.multiple_of(n * step, step), step)
+            gate = dot(gat[group(zz), :], eg[:, col])
+            value = dot(gat[group(zz), :], eu[:, col])
+            act[:, col] = (gate / (1.0 + jnp.exp(-gate)) * value * weight).astype(BF)
 
         @pl.loop(0, 4)
         def _(n):
-            ys[:, cols(n)] = dot(act[...], ed[:, cols(n)]).astype(BF)
-
-        for i, zz in enumerate(pair):
-            is_own = zz == z
-
-            @pl.loop(0, 4)
-            def _(n):
-                out = lax.dot_general(
-                    marks[i][1],
-                    ys[pl.ds(i * slots, slots), cols(n)],
-                    (((0,), (0,)), ((), ())),
-                    preferred_element_type=F32,
-                )
-                dst = pl.ds(pl.multiple_of(zz * tp, tp), tp)
-                if zz is order[0]:
-                    out = out + dot(sact[...], sd[:, cols(n)])
-                dd[dst, :, cols(n)] = out.astype(BF).reshape(tp, rows, tile)
+            out = dot(act[:, :depth], ed[:depth, cols(n)])
+            dst = pl.ds(pl.multiple_of(zz * tp, tp), tp)
+            dd[dst, :, cols(n)] = out.astype(BF).reshape(tp, rows, tile)
 
     def d_core(zz, xx):
         return rcopy(dd.at[block(zz, xx, 1 - c)], rc.at[zz, xx], rc_s.at[zz, xx], rc_r.at[zz, xx], pc)
@@ -416,43 +394,13 @@
         src = part_of(dd.at[block(zz, x, c)], p)
         return rcopy(src, part_of(zd.at[zz], p), zd_s.at[zz, p], zd_r.at[zz, p], down)
 
-    z_step(1)
-
-    x_step(order[0])
-    z_step(2)
-    core_step(order[0])
-    for name in ("sg", "su", "sd"):
-        loads[name].wait()
-    hidden = dot(gat[group(z), :], sgu[...])
-    gate, value = hidden[:, :half], hidden[:, half:]
-    sact[...] = (gate / (1.0 + jnp.exp(-gate)) * value).astype(BF)
-    for s in range(3, ep):
-        z_step(s)
-
-    m_x = rcopy(mp.at[(1 - x) * 2 + c], mrx, m_s.at[2], m_r.at[2], xn)
-    for xx in range(2):
-        m_core(xx).wait_recv()
-    mine = (1 - x) * 2 + c
-    mp[mine] = (mp[mine].astype(F32) + mrc[1 - x].astype(F32)).astype(BF)
-    m_x.start()
-
-    x_step(order[1])
-    core_step(order[1])
-    for name in ("eg", "eu", "ed"):
-        loads[name].wait()
-    for n in range(0, ep, 2):
-        pair = order[n : n + 2]
-        if n:
-            for zz in pair:
-                x_step(zz)
-            for zz in pair:
-                core_step(zz)
-        experts(pair)
-        for zz in pair[::-1]:
-            for xx in range(2):
-                d_core(zz, xx).start()
-
-    for zz in order[::-1]:
+    def compute(zz, depth):
+        core_step(zz)
+        experts(zz, depth)
+        for xx in range(2):
+            d_core(zz, xx).start()
+
+    def fold_core(zz):
         for xx in range(2):
             d_core(zz, xx).wait_recv()
         there = block(zz, 1 - x, c)
@@ -460,12 +408,7 @@
         for p in range(PARTS):
             d_x(zz, p).start()
 
-    m_x.wait_recv()
-    mixed = mp[t].astype(F32) + mrc[x].astype(F32) + mrx[...].astype(F32)
-    scale = lax.rsqrt(jnp.mean(mixed * mixed, axis=-1, keepdims=True) + EPSILON)
-    mixed_ref[...] = (mixed * scale * mgain[...]).astype(BF)
-
-    for zz in order[:0:-1]:
+    def fold_z(zz):
         here = block(zz, x, c)
         lower = zz < z
         for p in range(PARTS):
@@ -497,6 +440,58 @@
             def _():
                 d_up(zz, p).start()
 
+    lower_half = 2 * z < ep
+
+    def target(n):
+        found = 0
+        for edge in range((ep + 1) // 2):
+            ranked = sorted((l for l in range(ep) if l != edge), key=lambda l: (-abs(l - edge), l))
+            found = jnp.where(jnp.minimum(z, ep - 1 - z) == edge, ranked[n - 1], found)
+        return jnp.where(lower_half, found, ep - 1 - found)
+
+    m_x = rcopy(mp.at[(1 - x) * 2 + c], mrx, m_s.at[2], m_r.at[2], xn)
+
+    def mixer_send():
+        for xx in range(2):
+            m_core(xx).wait_recv()
+        mine = (1 - x) * 2 + c
+        mp[mine] = (mp[mine].astype(F32) + mrc[1 - x].astype(F32)).astype(BF)
+        m_x.start()
+
+    z_step(1)
+    x_step(order[0])
+    if ep > 2:
+        z_step(2)
+    core_step(order[0])
+    shared()
+    for name in ("eg", "eu", "ed"):
+        loads[name].wait()
+    experts(order[0], hid + half)
+    for xx in range(2):
+        d_core(order[0], xx).start()
+    x_step(order[1])
+    mixer()
+    for s in range(3, ep):
+        z_step(s)
+    for n in range(2, ep):
+        x_step(order[n])
+    for n in range(1, ep - 1):
+        compute(order[n], hid)
+        if n == 1:
+            fold_core(order[1])
+    compute(order[ep - 1], hid)
+    for n in range(ep - 1, 1 if ep > 2 else 0, -1):
+        fold_core(order[n])
+    mixer_send()
+    fold_core(order[0])
+    for n in range(1, ep):
+        fold_z(target(n))
+
+    m_x.wait_recv()
+    mixed = mp[t].astype(F32) + mrc[x].astype(F32) + mrx[...].astype(F32)
+    scale = lax.rsqrt(jnp.mean(mixed * mixed, axis=-1, keepdims=True) + EPSILON)
+    mixed_ref[...] = (mixed * scale * mgain[...]).astype(BF)
+
     here = block(z, x, c)
     for p in range(PARTS):
         band = pl.ds(p * deep, deep)
@@ -566,28 +561,26 @@
     rows, width = tok.shape
     count, columns = ig.shape
     experts = ep * tp
-    cap = (3 * rows * ids.shape[1] + 2 * experts - 1) // (2 * experts)
     names = -(-experts // 16) * 16
     hid = eg.shape[2]
     half = sd.shape[0]
-    any_spec = pl.BlockSpec(memory_space=pl.ANY)
+    any_spec = pl.BlockSpec(memory_space=pltpu.HBM)
     vmem = pl.BlockSpec(memory_space=pltpu.VMEM)
     dma = pltpu.SemaphoreType.DMA
     V = pltpu.VMEM
     return pl.pallas_call(
-        functools.partial(fused_kernel, ep, tp, cap),
-        out_shape=(jax.ShapeDtypeStruct((rows, width), BF), jax.ShapeDtypeStruct((rows, width), BF)),
+        functools.partial(fused_kernel, ep, tp),
+        out_shape=(V((rows, width), BF), V((rows, width), BF)),
         in_specs=[any_spec] * 3 + [vmem, any_spec, vmem, any_spec, vmem, vmem, vmem] + [any_spec] * 6,
         out_specs=(vmem, vmem),
         scratch_shapes=[
             V((count, columns), BF), V((count, columns), BF), V((count, columns), BF),
             V((columns, width), BF), V((rows, width), BF),
-            V((width, hid), BF), V((width, hid), BF), V((hid, width), BF),
-            V((width, 2 * half), BF), V((half, width), BF),
+            V((width, hid), BF), V((width, hid), BF), V((hid + half, width), BF),
+            V((width, 2 * half), BF),
             V((2, 16, columns), BF), V((count + 8, columns), F32), V((count, columns), BF),
             V((experts * rows, width), BF), V((experts, names, 128), BF),
-            V((2 * tp * cap, width), BF), V((2 * tp * cap, hid), BF), V((2 * tp * cap, width), BF),
-            V((tp * rows, half), BF),
+            V((tp * rows, hid + half), BF),
             V((experts, rows, width), BF), V((ep, 2, rows, width), BF), V((ep, rows, width), BF),
             V((ep, rows, width), BF), V((ep, rows, width), BF),
             V((tp, rows, width), BF), V((2, rows, width), BF), V((rows, width), BF),

time: 74.5 us -> 68.4 us (0.918)
  Pallas kernels: 69.8 us -> 66.2 us
  local copies, waits for them, and re-layouts: 3.34 us -> 1.41 us
    pallas_call x1, Pallas kernels: 69.8 us -> 66.2 us  [fused_on_device(): pl.pallas_call(functools.partial(fused_kernel, ep, tp), out_shape=(V((row...]
    unnamed x2, local copies, waits for them, and re-layouts: 3.34 us -> 1.41 us
where the time goes in v1:
time: 68.4 us; the launch traced here: 68.2 us
  Pallas kernels  66.2 us (97%)
  local copies, waits for them, and re-layouts  1.41 us (2%)
    pallas_call x1, Pallas kernels, fused_on_device(): pl.pallas_call(functools.partial(fused_kernel, ep, tp), out_shape=(V((row...  66.2 us
    unnamed x2, local copies, waits for them, and re-layouts  1.41 us

profile of v1, /device:TPU:0, one launch (start us, length us, event | category | flops | bytes accessed | tf_op | source)
XLA Modules:
  0.0 68.2 jit_solution(15150608927505828145)
XLA Ops:
  0.6 66.2 %shard_map.167 = (bf16[64,2048]{1,0:T(8,128)(2,1)S(1)}, bf16[64,2048]{1,0:T(8,128)(2,1)S(1)}) custom-call(bf16[256,512]{1,0:T(8,128)(2,1)} %og_h.1, bf16[256,512]{1,0:T(8,128)(2,1)} %ig_h.1, bf16[256,512]{1,0:T(8,128)(2,1)} %iv_h.1, bf16[3,2048]{1,0:T(4,128)(2,1)} %taps.1, bf16[512,2048]{1,0:T(8,128)(2,1)} %mo_h.1, f32[1,2048]{1,0:T(1,128)} %bitcast.4, ...), custom_call_target="tpu_custom_call" | custom-call | tf_op jit(solution)/shard_map/pallas_call | solution.py:571
  66.8 0.7 %copy.20 = bf16[64,2048]{1,0:T(8,128)(2,1)} copy(bf16[64,2048]{1,0:T(8,128)(2,1)S(1)} %get-tuple-element.2) | data formatting | bytes 524288
  67.5 0.7 %copy.21 = bf16[64,2048]{1,0:T(8,128)(2,1)} copy(bf16[64,2048]{1,0:T(8,128)(2,1)S(1)} %get-tuple-element.3) | data formatting | bytes 524288

commit v2 on v1

v2 whole, which is shorter than its diff:
```python
import functools
import jax
import jax.numpy as jnp
from jax import lax
from jax.experimental import pallas as pl
from jax.experimental.pallas import tpu as pltpu
from jax.sharding import PartitionSpec as P

EPSILON = 1e-06


def passed_along(array, axis, by):
    size = lax.axis_size(axis)
    pairs = [(i, i + by) for i in range(size) if 0 <= i + by < size]
    return lax.ppermute(array, axis, pairs)


def rms_scale(values, gains):
    return values * lax.rsqrt(jnp.mean(values * values, axis=-1, keepdims=True) + EPSILON) * gains


def on_device(
    outer_gate,
    inner_gate,
    inner_value,
    conv_taps,
    mixer_out,
    mixer_gain,
    moe_tokens,
    expert_gain,
    route_ids,
    route_weights,
    expert_gate,
    expert_up,
    expert_down,
    shared_gate,
    shared_up,
    shared_down,
):
    columns = inner_gate.shape[1]
    kernel = lax.dynamic_slice_in_dim(conv_taps, lax.axis_index("tp") * columns, columns, 1).astype(
        jnp.float32
    )
    before_gate, before_value = passed_along((inner_gate[-2:], inner_value[-2:]), "ep", 1)
    gate_rows = jnp.concatenate([before_gate, inner_gate], axis=0).astype(jnp.float32)
    value_rows = jnp.concatenate([before_value, inner_value], axis=0).astype(jnp.float32)
    product = gate_rows * value_rows
    filtered = kernel[0] * product[:-2] + kernel[1] * product[1:-1] + kernel[2] * product[2:]
    scaled = (outer_gate.astype(jnp.float32) * filtered).astype(jnp.bfloat16)
    normed = rms_scale(moe_tokens.astype(jnp.float32), expert_gain).astype(jnp.bfloat16)
    feature_width = normed.shape[1]
    piece = lax.all_gather(normed, "tp", axis=0, tiled=True)
    gate_value = jnp.dot(piece, shared_gate, preferred_element_type=jnp.float32)
    up_value = jnp.dot(piece, shared_up, preferred_element_type=jnp.float32)
    shared_act = (jax.nn.silu(gate_value) * up_value).astype(jnp.bfloat16)
    mixer_part = jnp.dot(scaled, mixer_out, preferred_element_type=jnp.float32)
    shared_part = jnp.dot(shared_act, shared_down, preferred_element_type=jnp.float32)
    both_sums = lax.psum_scatter(
        jnp.concatenate([mixer_part, shared_part], axis=1).astype(jnp.bfloat16),
        "tp",
        scatter_dimension=0,
        tiled=True,
    ).astype(jnp.float32)
    mixed_rows = rms_scale(both_sums[:, :feature_width], mixer_gain).astype(jnp.bfloat16)
    shared_out = both_sums[:, feature_width:]
    row_count, top_count = route_ids.shape
    ep_count = lax.axis_size("ep")
    tp_count = lax.axis_size("tp")
    expert_count = ep_count * tp_count
    capacity = (3 * row_count * top_count + 2 * expert_count - 1) // (2 * expert_count)
    flat_ids = route_ids.reshape(-1)
    onehot = (flat_ids[:, None] == jnp.arange(expert_count, dtype=jnp.int32)[None, :]).astype(
        jnp.int32
    )
    slot_rank = jnp.sum(
        (jnp.cumsum(onehot, axis=0, dtype=jnp.int32) - onehot) * onehot, axis=1, dtype=jnp.int32
    )
    target = flat_ids * capacity + slot_rank
    token_of = jnp.arange(flat_ids.shape[0], dtype=jnp.int32) // top_count
    slot_token = jnp.zeros((expert_count * capacity,), jnp.int32).at[target].set(token_of)
    outgoing = normed[slot_token].reshape(expert_count, capacity, feature_width)
    arrived = lax.all_to_all(outgoing, ("ep", "tp"), split_axis=0, concat_axis=0, tiled=True)
    flat_in = arrived.reshape(expert_count * capacity, feature_width)
    gate_value = jnp.dot(flat_in, expert_gate[0], preferred_element_type=jnp.float32)
    up_value = jnp.dot(flat_in, expert_up[0], preferred_element_type=jnp.float32)
    active = (jax.nn.silu(gate_value) * up_value).astype(jnp.bfloat16)
    result = jnp.dot(active, expert_down[0], preferred_element_type=jnp.float32).astype(
        jnp.bfloat16
    )
    returned = lax.all_to_all(
        result.reshape(expert_count, capacity, feature_width),
        ("ep", "tp"),
        split_axis=0,
        concat_axis=0,
        tiled=True,
    )
    picked = returned.reshape(expert_count * capacity, feature_width)[target].astype(jnp.float32)
    weights = route_weights.reshape(-1)
    routed = jnp.sum(
        (weights[:, None] * picked).reshape(row_count, top_count, feature_width), axis=1
    )
    expert_rows = (shared_out + routed).astype(jnp.bfloat16)
    return (mixed_rows, expert_rows)


MESH = pl.DeviceIdType.MESH
BF = jnp.bfloat16
F32 = jnp.float32
CHUNKS = 2
PARTS = 4
HALVES = 2
PIECES = (CHUNKS,) + tuple(range(CHUNKS))


def dot(a, b):
    return jnp.dot(a, b, preferred_element_type=F32)


def dot_rows(a, b):
    return lax.dot_general(a, b, (((0,), (0,)), ((), ())), preferred_element_type=F32)


def fused_kernel(
    ep, tp, cap, slot,
    og_h, ig_h, iv_h, taps, mo_h, mgain, tok_h, egain, ids, wts, eg_h, eu_h, ed_h, sg_h, su_h, sd_h,
    mixed_ref, rows_ref,
    og, ig, iv, mo, tok, eg, eu, ed, sgu, halo, pbuf, scaled,
    gat, tab, act, dd, packed, spread, rc, back, rx, edge_in, last_in, mp, mrc, mrx,
    load_sem, halo_sem, gz_r, gz_su, gz_sd, gx_r, gx_s, gc_r, gc_s, px_r, px_s,
    rc_r, rc_s, q_r, q_s, rx_r, rx_s, e_r, e_s, f_r, f_s, m_r, m_s,
):
    z = lax.axis_index("ep")
    t = lax.axis_index("tp")
    g = lax.axis_index("grp")
    x = t // 2
    c = t % 2
    rows = tok.shape[0]
    width = tok.shape[1]
    columns = ig.shape[1]
    sub = rows // CHUNKS
    up = (g, z + 1, t)
    down = (g, z - 1, t)
    xn = (g, z, (1 - x) * 2 + c)
    pc = (g, z, x * 2 + 1 - c)
    xd = (g, z, (1 - x) * 2 + 1 - c)
    z2 = (g, (z + 2) % ep, t)
    is_edge = jnp.logical_or(z == 0, z == ep - 1)
    inner = jnp.where(2 * z < ep, z + 1, z - 1)
    outer = jnp.where(2 * z < ep, z - 1, z + 1)
    has_up = z < ep - 1
    has_down = z > 0

    loads = {}

    def load(name, src, dst):
        copy = pltpu.make_async_copy(src, dst, load_sem.at[len(loads)])
        copy.start()
        loads[name] = copy

    half = sd_h.shape[0]
    hid = eg.shape[1]
    load("tok", tok_h, tok)
    load("ig", ig_h, ig)
    load("iv", iv_h, iv)
    load("og", og_h, og)
    load("mo", mo_h, mo)
    load("sg", sg_h, sgu.at[:, pl.ds(0, half)])
    load("su", su_h, sgu.at[:, pl.ds(half, half)])
    load("sd", sd_h, ed.at[pl.ds(hid, half), :])
    load("eg", eg_h.at[0], eg)
    load("eu", eu_h.at[0], eu)
    load("ed", ed_h.at[0], ed.at[pl.ds(0, hid), :])

    barrier = pltpu.get_barrier_semaphore()
    for peer in (xn, pc, xd, z2):
        pl.semaphore_signal(barrier, inc=1, device_id=peer, device_id_type=MESH)

    @pl.when(has_up)
    def _():
        pl.semaphore_signal(barrier, inc=1, device_id=up, device_id_type=MESH)

    @pl.when(has_down)
    def _():
        pl.semaphore_signal(barrier, inc=1, device_id=down, device_id_type=MESH)

    def rcopy(src, dst, ssem, rsem, peer):
        return pltpu.make_async_remote_copy(
            src_ref=src, dst_ref=dst, send_sem=ssem, recv_sem=rsem, device_id=peer, device_id_type=MESH
        )

    def block(zz, side, cc):
        return (zz * 2 + side) * 2 + cc

    def lines(zz, side, cc):
        return pl.ds(pl.multiple_of(block(zz, side, cc) * rows, rows), rows)

    def few(zz, cc):
        return pl.ds(pl.multiple_of(block(zz, 1, 0) * rows + cc * slot, slot), cap)

    def slots_of(cc):
        return pl.ds(pl.multiple_of(cc * slot, slot), cap)

    def piece(zz, side, cc, k):
        if k == CHUNKS:
            return tab.at[block(zz, side, cc)]
        return gat.at[pl.ds(pl.multiple_of(block(zz, side, cc) * rows + k * sub, sub), sub), :]

    def c_up(zz, k):
        return rcopy(piece(zz, 0, c, k), piece(zz, 0, c, k), gz_su.at[zz, k], gz_r.at[zz, k], up)

    def c_down(zz, k):
        return rcopy(piece(zz, 0, c, k), piece(zz, 0, c, k), gz_sd.at[zz, k], gz_r.at[zz, k], down)

    def c_x(k):
        return rcopy(piece(z, 0, c, k), piece(z, 1, c, k), gx_s.at[k], gx_r.at[k], xn)

    def core_pair(zz, side, cc):
        names = tab.at[block(zz, side, cc)]
        body = gat.at[lines(zz, side, cc), :]
        return (
            rcopy(body, body, gc_s.at[zz, side, 0], gc_r.at[zz, side, 0], pc),
            rcopy(names, names, gc_s.at[zz, side, 1], gc_r.at[zz, side, 1], pc),
        )

    def core_start(zz, side):
        for copy in core_pair(zz, side, c):
            copy.start()

    def few_pair(zz):
        return (
            rcopy(packed.at[zz, slots_of(c), :], gat.at[few(zz, c), :], px_s.at[zz, 0], px_r.at[zz, 0], xn),
            rcopy(packed.at[zz, slots_of(1 - c), :], gat.at[few(zz, c), :], px_s.at[zz, 1], px_r.at[zz, 1], xd),
        )

    for zz in range(ep):
        for e in range(2):
            back[zz, pl.ds(e * slot + cap, slot - cap), :] = jnp.zeros((slot - cap, width), BF)

    loads["tok"].wait()
    name_i = lax.broadcasted_iota(jnp.int32, (tab.shape[1], rows), 0)
    table = jnp.zeros((tab.shape[1], rows), F32)
    for k in range(ids.shape[0]):
        table = table + jnp.where(ids[k : k + 1, :] == name_i, wts[k : k + 1, :], 0.0)
    tab[block(z, 0, c)] = jnp.zeros(tab.shape[1:], BF)
    tab[block(z, 0, c), :, :rows] = table.astype(BF)
    v = tok[...].astype(F32)
    v = v * lax.rsqrt(jnp.mean(v * v, axis=-1, keepdims=True) + EPSILON) * egain[...]
    gat[lines(z, 0, c), :] = v.astype(BF)

    pl.semaphore_wait(barrier, 4 + jnp.minimum(z, 1) + jnp.minimum(ep - 1 - z, 1))

    loads["ig"].wait()
    loads["iv"].wait()
    tail = ig.shape[0] - halo.shape[1]
    edge = halo.shape[1]
    h_gate = rcopy(ig.at[pl.ds(tail, edge)], halo.at[0], halo_sem.at[0], halo_sem.at[1], up)
    h_value = rcopy(iv.at[pl.ds(tail, edge)], halo.at[1], halo_sem.at[2], halo_sem.at[3], up)

    @pl.when(has_up)
    def _():
        h_gate.start()
        h_value.start()

    for k in PIECES:
        @pl.when(has_up)
        def _():
            c_up(z, k).start()

        @pl.when(has_down)
        def _():
            c_down(z, k).start()

        c_x(k).start()
    core_start(z, 0)

    count = ig.shape[0]
    tile = width // PARTS

    def cols(n):
        return pl.ds(pl.multiple_of(n * tile, tile), tile)

    def m_core(xx):
        return rcopy(mp.at[xx * 2 + 1 - c], mrc.at[xx], m_s.at[xx], m_r.at[xx], pc)

    def mixer():
        pbuf[8:, :] = ig[...].astype(F32) * iv[...].astype(F32)

        @pl.when(jnp.logical_not(has_down))
        def _():
            pbuf[:8, :] = jnp.zeros((8, columns), F32)

        @pl.when(has_down)
        def _():
            h_gate.wait_recv()
            h_value.wait_recv()
            pbuf[:8, :] = halo[0, edge - 8 :, :].astype(F32) * halo[1, edge - 8 :, :].astype(F32)

        loads["og"].wait()
        tap = taps[:, pl.ds(pl.multiple_of(t * columns, columns), columns)].astype(F32)
        filtered = (
            tap[0:1] * pbuf[6 : 6 + count, :] + tap[1:2] * pbuf[7 : 7 + count, :] + tap[2:3] * pbuf[8 : 8 + count, :]
        )
        scaled[...] = (og[...].astype(F32) * filtered).astype(BF)
        loads["mo"].wait()
        @pl.loop(0, 4)
        def _(n):
            part = dot(scaled[...], mo[:, cols(n)]).astype(BF)
            mp[:, :, cols(n)] = part.reshape(tp, rows, tile)

        for xx in range(2):
            m_core(xx).start()

    lanes = tab.shape[2]
    name_of = lax.broadcasted_iota(jnp.int32, (tab.shape[1], lanes), 0)
    before = (
        lax.broadcasted_iota(jnp.int32, (lanes, lanes), 0) < lax.broadcasted_iota(jnp.int32, (lanes, lanes), 1)
    ).astype(BF)
    slot_i = lax.broadcasted_iota(jnp.int32, (slot, lanes), 0)
    diagonal = lax.broadcasted_iota(jnp.int32, (rows, lanes), 0) == lax.broadcasted_iota(
        jnp.int32, (rows, lanes), 1
    )
    expert = z * tp + t

    def line_of(name, block_id):
        return jnp.sum(jnp.where(name_of == name, tab[block_id].astype(F32), 0.0), axis=0, keepdims=True)

    def weight_column(block_id):
        return jnp.sum(jnp.where(diagonal, line_of(expert, block_id), 0.0), axis=1, keepdims=True)

    def compact(zz):
        marks = []
        for e in range(2):
            weight = line_of(z * tp + (1 - x) * 2 + e, block(zz, 0, c))
            named = weight > 0
            ahead = dot(jnp.broadcast_to(named, (8, lanes)).astype(F32).astype(BF), before)[0:1]
            hit = jnp.logical_and(slot_i == ahead.astype(jnp.int32), named)
            marks.append(hit.astype(F32))
            spread[zz, pl.ds(e * slot, slot), :] = jnp.where(hit, weight, 0.0).astype(BF)
        mark = jnp.concatenate(marks, axis=0).astype(BF)[:, :rows]

        @pl.loop(0, PARTS)
        def _(n):
            packed[zz, :, cols(n)] = dot(mark, gat[lines(zz, 0, c), cols(n)]).astype(BF)

        for copy in few_pair(zz):
            copy.start()

    def z_step(s):
        for k in PIECES:
            @pl.when(z >= s)
            def _():
                c_up(z - s, k).wait_recv()

                @pl.when(has_up)
                def _():
                    c_up(z - s, k).start()

            @pl.when(z + s < ep)
            def _():
                c_down(z + s, k).wait_recv()

                @pl.when(has_down)
                def _():
                    c_down(z + s, k).start()

        @pl.when(z >= s)
        def _():
            core_start(z - s, 0)

        @pl.when(z + s < ep)
        def _():
            core_start(z + s, 0)

    def compacts(s):
        @pl.when(z >= s)
        def _():
            compact(z - s)

        @pl.when(z + s < ep)
        def _():
            compact(z + s)

    def own_x():
        for k in PIECES:
            c_x(k).wait_recv()
        core_start(z, 1)

    def core_step(zz, sides):
        for side in range(sides):
            for copy in core_pair(zz, side, 1 - c):
                copy.wait_recv()
        if sides == 1:
            for copy in few_pair(zz):
                copy.wait_recv()

    def nth(n):
        near = jnp.minimum(z, ep - 1 - z)
        d = (n + 1) // 2
        side = z - d if n % 2 else z + d
        far = jnp.where(z < ep - 1 - z, n, ep - 1 - n)
        return jnp.where(n <= 2 * near, side, far)

    order = [nth(n) for n in range(ep)]

    def shared():
        for name in ("sg", "su", "sd"):
            loads[name].wait()
        own = pl.ds(pl.multiple_of(block(z, 0, 0) * rows, tp * rows), tp * rows)
        hidden = dot(gat[own, :], sgu[...])
        gate, value = hidden[:, :half], hidden[:, half:]
        act[:, hid:] = (gate / (1.0 + jnp.exp(-gate)) * value).astype(BF)

    def experts(zz, sides):
        depth = hid + half if sides == 2 else hid
        weights = [weight_column(block(zz, side, cc)) for side in range(sides) for cc in range(2)]
        if sides == 1:
            weights.append(jnp.ones((2 * slot, 1), F32))
        weight = jnp.concatenate(weights, axis=0)
        amount = weight.shape[0]
        span = pl.ds(pl.multiple_of(block(zz, 0, 0) * rows, tp * rows), amount)
        step = 256 if hid % 256 == 0 else hid

        @pl.loop(0, hid // step)
        def _(n):
            col = pl.ds(pl.multiple_of(n * step, step), step)
            gate = dot(gat[span, :], eg[:, col])
            value = dot(gat[span, :], eu[:, col])
            act[:amount, col] = (gate / (1.0 + jnp.exp(-gate)) * value * weight).astype(BF)

        @pl.loop(0, PARTS)
        def _(n):
            dd[span, cols(n)] = dot(act[:amount, :depth], ed[:depth, cols(n)]).astype(BF)

    def d_core(zz, side):
        at = zz if side == 0 else ep
        return rcopy(dd.at[lines(zz, side, 1 - c), :], rc.at[at], rc_s.at[at], rc_r.at[at], pc)

    wide = width // HALVES

    def d_few(zz, h):
        part = pl.ds(h * wide, wide)
        return (
            rcopy(
                dd.at[few(zz, c), part], back.at[zz, slots_of(c), part],
                q_s.at[zz, h, 0], q_r.at[zz, h, 0], xn,
            ),
            rcopy(
                dd.at[few(zz, 1 - c), part], back.at[zz, slots_of(c), part],
                q_s.at[zz, h, 1], q_r.at[zz, h, 1], xd,
            ),
        )

    def d_x(p):
        return rcopy(dd.at[lines(z, 1, c), cols(p)], rx.at[:, cols(p)], rx_s.at[p], rx_r.at[p], xn)

    def to_inner(zz, p):
        src = dd.at[lines(zz, 0, c), cols(p)]
        return rcopy(src, edge_in.at[zz, :, cols(p)], e_s.at[zz, p], e_r.at[zz, p], (g, inner, t))

    def to_owner(zz, p):
        owner_is_edge = jnp.logical_or(zz == 0, zz == ep - 1)
        place = jnp.where(jnp.logical_and(owner_is_edge, zz == outer), 0, 1)
        src = dd.at[lines(zz, 0, c), cols(p)]
        return rcopy(src, last_in.at[place, :, cols(p)], f_s.at[zz, p], f_r.at[place, p], (g, zz, t))

    def last_arrival(place, p):
        here = last_in.at[place, :, cols(p)]
        return rcopy(here, here, f_s.at[place, p], f_r.at[place, p], xn)

    def compute(zz):
        core_step(zz, 1)
        experts(zz, 1)
        d_core(zz, 0).start()
        for h in range(HALVES):
            for copy in d_few(zz, h):
                copy.start()

    def fold_core():
        d_core(z, 1).wait_recv()
        there = lines(z, 1, c)
        dd[there, :] = (dd[there, :].astype(F32) + rc[ep].astype(F32)).astype(BF)
        for p in range(PARTS):
            d_x(p).start()

    def fold_z(zz):
        here = lines(zz, 0, c)
        d_core(zz, 0).wait_recv()
        for p in range(PARTS):
            band = cols(p)
            if p % (PARTS // HALVES) == 0:
                for copy in d_few(zz, p // (PARTS // HALVES)):
                    copy.wait_recv()
            so_far = (
                dd[here, band].astype(F32)
                + rc[zz, :, band].astype(F32)
                + dot_rows(spread[zz], back[zz, :, band])[:rows]
            )

            @pl.when(jnp.logical_or(is_edge, zz == outer))
            def _():
                dd[here, band] = so_far.astype(BF)

            @pl.when(jnp.logical_not(jnp.logical_or(is_edge, zz == outer)))
            def _():
                to_inner(zz, p).wait_recv()
                dd[here, band] = (so_far + edge_in[zz, :, band].astype(F32)).astype(BF)

            @pl.when(is_edge)
            def _():
                to_inner(zz, p).start()

            @pl.when(jnp.logical_not(is_edge))
            def _():
                to_owner(zz, p).start()

    def target(n):
        edge_first, inner_first = ((2, 3, 1), (0, 2, 3))
        found = jnp.where(is_edge, edge_first[n - 1], inner_first[n - 1])
        return jnp.where(2 * z < ep, found, ep - 1 - found)

    def m_x(h):
        part = pl.ds(h * wide, wide)
        return rcopy(mp.at[(1 - x) * 2 + c, :, part], mrx.at[:, part], m_s.at[2 + h], m_r.at[2 + h], xn)

    def mixer_fold():
        for xx in range(2):
            m_core(xx).wait_recv()
        mine = (1 - x) * 2 + c
        mp[mine] = (mp[mine].astype(F32) + mrc[1 - x].astype(F32)).astype(BF)

    def mixer_send(h):
        m_x(h).start()

    z_step(1)
    compacts(1)
    own_x()
    mixer()
    z_step(2)
    compacts(2)
    for name in ("eg", "eu", "ed"):
        loads[name].wait()
    compute(order[1])
    z_step(3)
    compacts(3)
    core_step(z, 2)
    shared()
    experts(z, 2)
    for side in range(2):
        d_core(z, side).start()
    compute(order[2])
    compute(order[3])
    mixer_fold()
    mixer_send(0)
    fold_z(target(1))
    mixer_send(1)
    fold_core()
    fold_z(target(2))
    fold_z(target(3))

    for h in range(HALVES):
        m_x(h).wait_recv()
    mixed = mp[t].astype(F32) + mrc[x].astype(F32) + mrx[...].astype(F32)
    scale = lax.rsqrt(jnp.mean(mixed * mixed, axis=-1, keepdims=True) + EPSILON)
    mixed_ref[...] = (mixed * scale * mgain[...]).astype(BF)

    here = lines(z, 0, c)
    d_core(z, 0).wait_recv()
    for p in range(PARTS):
        band = cols(p)
        d_x(p).wait_recv()
        total = dd[here, band].astype(F32) + rc[z, :, band].astype(F32) + rx[:, band].astype(F32)

        last_arrival(1, p).wait_recv()
        total = total + last_in[1, :, band].astype(F32)

        @pl.when(is_edge)
        def _():
            last_arrival(0, p).wait_recv()
            rows_ref[:, band] = (total + last_in[0, :, band].astype(F32)).astype(BF)

        @pl.when(jnp.logical_not(is_edge))
        def _():
            to_inner(z, p).wait_recv()
            rows_ref[:, band] = (total + edge_in[z, :, band].astype(F32)).astype(BF)

    @pl.when(has_up)
    def _():
        h_gate.wait_send()
        h_value.wait_send()

    for k in PIECES:
        c_x(k).wait_send()
    for p in range(PARTS):
        d_x(p).wait_send()
    for copy in core_pair(z, 1, c):
        copy.wait_send()
    d_core(z, 1).wait_send()

    for zz in range(ep):
        @pl.when(jnp.logical_and(has_up, zz <= z))
        def _():
            for k in PIECES:
                c_up(zz, k).wait_send()

        @pl.when(jnp.logical_and(has_down, zz >= z))
        def _():
            for k in PIECES:
                c_down(zz, k).wait_send()

        for copy in core_pair(zz, 0, c):
            copy.wait_send()
        d_core(zz, 0).wait_send()

        @pl.when(zz != z)
        def _():
            for copy in few_pair(zz):
                copy.wait_send()
            for h in range(HALVES):
                for copy in d_few(zz, h):
                    copy.wait_send()

        @pl.when(jnp.logical_and(zz != z, is_edge))
        def _():
            for p in range(PARTS):
                to_inner(zz, p).wait_send()

        @pl.when(jnp.logical_and(zz != z, jnp.logical_not(is_edge)))
        def _():
            for p in range(PARTS):
                to_owner(zz, p).wait_send()

    for xx in range(2):
        m_core(xx).wait_send()
    for h in range(HALVES):
        m_x(h).wait_send()


def fused_on_device(ep, tp, *args):
    (og, ig, iv, taps, mo, mgain, tok, egain, ids, wts, eg, eu, ed, sg, su, sd) = args
    rows, width = tok.shape
    count, columns = ig.shape
    experts = ep * tp
    cap = (3 * rows * ids.shape[1] + 2 * experts - 1) // (2 * experts)
    cap = -(-cap // 8) * 8
    slot = -(-cap // 32) * 32
    names = -(-experts // 16) * 16
    hid = eg.shape[2]
    half = sd.shape[0]
    any_spec = pl.BlockSpec(memory_space=pltpu.HBM)
    vmem = pl.BlockSpec(memory_space=pltpu.VMEM)
    dma = pltpu.SemaphoreType.DMA
    V = pltpu.VMEM
    return pl.pallas_call(
        functools.partial(fused_kernel, ep, tp, cap, slot),
        out_shape=(V((rows, width), BF), V((rows, width), BF)),
        in_specs=[any_spec] * 3 + [vmem, any_spec, vmem, any_spec, vmem, vmem, vmem] + [any_spec] * 6,
        out_specs=(vmem, vmem),
        scratch_shapes=[
            V((count, columns), BF), V((count, columns), BF), V((count, columns), BF),
            V((columns, width), BF), V((rows, width), BF),
            V((width, hid), BF), V((width, hid), BF), V((hid + half, width), BF),
            V((width, 2 * half), BF),
            V((2, 16, columns), BF), V((count + 8, columns), F32), V((count, columns), BF),
            V((experts * rows, width), BF), V((experts, names, 128), BF),
            V((tp * rows, hid + half), BF), V((experts * rows, width), BF),
            V((ep, 2 * slot, width), BF), V((ep, 2 * slot, 128), BF),
            V((ep + 1, rows, width), BF), V((ep, 2 * slot, width), BF), V((rows, width), BF),
            V((ep, rows, width), BF), V((2, rows, width), BF),
            V((tp, rows, width), BF), V((2, rows, width), BF), V((rows, width), BF),
            dma((11,)), dma((4,)),
            dma((ep, CHUNKS + 1)), dma((ep, CHUNKS + 1)), dma((ep, CHUNKS + 1)),
            dma((CHUNKS + 1,)), dma((CHUNKS + 1,)), dma((ep, 2, 2)), dma((ep, 2, 2)),
            dma((ep, 2)), dma((ep, 2)),
            dma((ep + 1,)), dma((ep + 1,)), dma((ep, HALVES, 2)), dma((ep, HALVES, 2)),
            dma((PARTS,)), dma((PARTS,)),
            dma((ep, PARTS)), dma((ep, PARTS)), dma((2, PARTS)), dma((ep, PARTS)),
            dma((2 + HALVES,)), dma((2 + HALVES,)),
        ],
        compiler_params=pltpu.CompilerParams(
            collective_id=0, has_side_effects=True, vmem_limit_bytes=60 * 1024 * 1024
        ),
    )(
        og, ig, iv, taps, mo, mgain.reshape(1, -1), tok, egain.reshape(1, -1), ids.T, wts.T, eg, eu, ed, sg, su, sd
    )


def plan(mesh):
    ep, tp = mesh.shape["ep"], mesh.shape["tp"]
    if tp == 4 and ep == 4:
        return functools.partial(fused_on_device, ep, tp)
    return on_device


def solution(mesh):
    return jax.shard_map(
        plan(mesh),
        mesh=mesh,
        in_specs=(
            P(("grp", "ep"), "tp"),
            P(("grp", "ep"), "tp"),
            P(("grp", "ep"), "tp"),
            P(),
            P("tp", None),
            P(),
            P(("grp", "ep", "tp"), None),
            P(),
            P(("grp", "ep", "tp"), None),
            P(("grp", "ep", "tp"), None),
            P(("ep", "tp"), None, None),
            P(("ep", "tp"), None, None),
            P(("ep", "tp"), None, None),
            P(None, "tp"),
            P(None, "tp"),
            P("tp", None),
        ),
        out_specs=(P(("grp", "ep", "tp"), None), P(("grp", "ep", "tp"), None)),
        check_vma=False,
    )
```

time: 68.4 us -> 58.5 us (0.86)
  Pallas kernels: 66.2 us -> 56.1 us
    pallas_call x1, Pallas kernels: 66.2 us -> 56.1 us  [fused_on_device(): pl.pallas_call(functools.partial(fused_kernel, ep, tp, cap, slot), out_sh...]
where the time goes in v2:
time: 58.5 us; the launch traced here: 58.2 us
  Pallas kernels  56.1 us (96%)
  local copies, waits for them, and re-layouts  1.41 us (2%)
  between operations  0.65 us (1%)
    pallas_call x1, Pallas kernels, fused_on_device(): pl.pallas_call(functools.partial(fused_kernel, ep, tp, cap, slot), out_sh...  56.1 us
    unnamed x2, local copies, waits for them, and re-layouts  1.41 us

profile of v2, /device:TPU:0, one launch (start us, length us, event | category | flops | bytes accessed | tf_op | source)
XLA Modules:
  0.0 58.2 jit_solution(17478440544674976290)
XLA Ops:
  0.6 56.1 %shard_map.167 = (bf16[64,2048]{1,0:T(8,128)(2,1)S(1)}, bf16[64,2048]{1,0:T(8,128)(2,1)S(1)}) custom-call(bf16[256,512]{1,0:T(8,128)(2,1)} %og_h.1, bf16[256,512]{1,0:T(8,128)(2,1)} %ig_h.1, bf16[256,512]{1,0:T(8,128)(2,1)} %iv_h.1, bf16[3,2048]{1,0:T(4,128)(2,1)} %taps.1, bf16[512,2048]{1,0:T(8,128)(2,1)} %mo_h.1, f32[1,2048]{1,0:T(1,128)} %bitcast.4, ...), custom_call_target="tpu_custom_call" | custom-call | tf_op jit(solution)/shard_map/pallas_call | solution.py:653
  56.8 0.7 %copy.20 = bf16[64,2048]{1,0:T(8,128)(2,1)} copy(bf16[64,2048]{1,0:T(8,128)(2,1)S(1)} %get-tuple-element.2) | data formatting | bytes 524288
  57.5 0.7 %copy.21 = bf16[64,2048]{1,0:T(8,128)(2,1)} copy(bf16[64,2048]{1,0:T(8,128)(2,1)S(1)} %get-tuple-element.3) | data formatting | bytes 524288

commit v3 on v2

--- a/solution.py
+++ b/solution.py
@@ -126,8 +126,7 @@
     mixed_ref, rows_ref,
     og, ig, iv, mo, tok, eg, eu, ed, sgu, halo, pbuf, scaled,
     gat, tab, act, dd, packed, spread, rc, back, rx, edge_in, last_in, mp, mrc, mrx,
-    load_sem, halo_sem, gz_r, gz_su, gz_sd, gx_r, gx_s, gc_r, gc_s, px_r, px_s,
-    rc_r, rc_s, q_r, q_s, rx_r, rx_s, e_r, e_s, f_r, f_s, m_r, m_s,
+    load_sem, halo_sem, gz_r, gx_r, gc_r, px_r, rc_r, q_r, rx_r, e_r, f_r, m_r, sent,
 ):
     z = lax.axis_index("ep")
     t = lax.axis_index("tp")
@@ -188,6 +187,9 @@
             src_ref=src, dst_ref=dst, send_sem=ssem, recv_sem=rsem, device_id=peer, device_id_type=MESH
         )
 
+    def arrived(ref, sem):
+        rcopy(ref, ref, sent.at[0], sem, xn).wait_recv()
+
     def block(zz, side, cc):
         return (zz * 2 + side) * 2 + cc
 
@@ -206,20 +208,21 @@
         return gat.at[pl.ds(pl.multiple_of(block(zz, side, cc) * rows + k * sub, sub), sub), :]
 
     def c_up(zz, k):
-        return rcopy(piece(zz, 0, c, k), piece(zz, 0, c, k), gz_su.at[zz, k], gz_r.at[zz, k], up)
+        return rcopy(piece(zz, 0, c, k), piece(zz, 0, c, k), sent.at[0], gz_r.at[zz, k], up)
 
     def c_down(zz, k):
-        return rcopy(piece(zz, 0, c, k), piece(zz, 0, c, k), gz_sd.at[zz, k], gz_r.at[zz, k], down)
+        return rcopy(piece(zz, 0, c, k), piece(zz, 0, c, k), sent.at[0], gz_r.at[zz, k], down)
 
     def c_x(k):
-        return rcopy(piece(z, 0, c, k), piece(z, 1, c, k), gx_s.at[k], gx_r.at[k], xn)
+        return rcopy(piece(z, 0, c, k), piece(z, 1, c, k), sent.at[0], gx_r.at[k], xn)
 
     def core_pair(zz, side, cc):
         names = tab.at[block(zz, side, cc)]
         body = gat.at[lines(zz, side, cc), :]
+        at = zz if side == 0 else ep
         return (
-            rcopy(body, body, gc_s.at[zz, side, 0], gc_r.at[zz, side, 0], pc),
-            rcopy(names, names, gc_s.at[zz, side, 1], gc_r.at[zz, side, 1], pc),
+            rcopy(body, body, sent.at[0], gc_r.at[at, 0], pc),
+            rcopy(names, names, sent.at[0], gc_r.at[at, 1], pc),
         )
 
     def core_start(zz, side):
@@ -228,8 +231,8 @@
 
     def few_pair(zz):
         return (
-            rcopy(packed.at[zz, slots_of(c), :], gat.at[few(zz, c), :], px_s.at[zz, 0], px_r.at[zz, 0], xn),
-            rcopy(packed.at[zz, slots_of(1 - c), :], gat.at[few(zz, c), :], px_s.at[zz, 1], px_r.at[zz, 1], xd),
+            rcopy(packed.at[zz, slots_of(c), :], gat.at[few(zz, c), :], sent.at[1], px_r.at[zz], xn),
+            rcopy(packed.at[zz, slots_of(1 - c), :], gat.at[few(zz, c), :], sent.at[1], px_r.at[zz], xd),
         )
 
     for zz in range(ep):
@@ -253,8 +256,8 @@
     loads["iv"].wait()
     tail = ig.shape[0] - halo.shape[1]
     edge = halo.shape[1]
-    h_gate = rcopy(ig.at[pl.ds(tail, edge)], halo.at[0], halo_sem.at[0], halo_sem.at[1], up)
-    h_value = rcopy(iv.at[pl.ds(tail, edge)], halo.at[1], halo_sem.at[2], halo_sem.at[3], up)
+    h_gate = rcopy(ig.at[pl.ds(tail, edge)], halo.at[0], sent.at[3], halo_sem.at[0], up)
+    h_value = rcopy(iv.at[pl.ds(tail, edge)], halo.at[1], sent.at[3], halo_sem.at[1], up)
 
     @pl.when(has_up)
     def _():
@@ -280,7 +283,7 @@
         return pl.ds(pl.multiple_of(n * tile, tile), tile)
 
     def m_core(xx):
-        return rcopy(mp.at[xx * 2 + 1 - c], mrc.at[xx], m_s.at[xx], m_r.at[xx], pc)
+        return rcopy(mp.at[xx * 2 + 1 - c], mrc.at[xx], sent.at[2], m_r.at[0], pc)
 
     def mixer():
         pbuf[8:, :] = ig[...].astype(F32) * iv[...].astype(F32)
@@ -302,7 +305,7 @@
         )
         scaled[...] = (og[...].astype(F32) * filtered).astype(BF)
         loads["mo"].wait()
-        @pl.loop(0, 4)
+        @pl.loop(0, PARTS, unroll=True)
         def _(n):
             part = dot(scaled[...], mo[:, cols(n)]).astype(BF)
             mp[:, :, cols(n)] = part.reshape(tp, rows, tile)
@@ -338,7 +341,7 @@
             spread[zz, pl.ds(e * slot, slot), :] = jnp.where(hit, weight, 0.0).astype(BF)
         mark = jnp.concatenate(marks, axis=0).astype(BF)[:, :rows]
 
-        @pl.loop(0, PARTS)
+        @pl.loop(0, PARTS, unroll=True)
         def _(n):
             packed[zz, :, cols(n)] = dot(mark, gat[lines(zz, 0, c), cols(n)]).astype(BF)
 
@@ -390,8 +393,7 @@
             for copy in core_pair(zz, side, 1 - c):
                 copy.wait_recv()
         if sides == 1:
-            for copy in few_pair(zz):
-                copy.wait_recv()
+            arrived(gat.at[pl.ds(pl.multiple_of(block(zz, 1, 0) * rows, rows), 2 * cap), :], px_r.at[zz])
 
     def nth(n):
         near = jnp.minimum(z, ep - 1 - z)
@@ -420,20 +422,20 @@
         span = pl.ds(pl.multiple_of(block(zz, 0, 0) * rows, tp * rows), amount)
         step = 256 if hid % 256 == 0 else hid
 
-        @pl.loop(0, hid // step)
+        @pl.loop(0, hid // step, unroll=True)
         def _(n):
             col = pl.ds(pl.multiple_of(n * step, step), step)
             gate = dot(gat[span, :], eg[:, col])
             value = dot(gat[span, :], eu[:, col])
             act[:amount, col] = (gate / (1.0 + jnp.exp(-gate)) * value * weight).astype(BF)
 
-        @pl.loop(0, PARTS)
+        @pl.loop(0, PARTS, unroll=True)
         def _(n):
             dd[span, cols(n)] = dot(act[:amount, :depth], ed[:depth, cols(n)]).astype(BF)
 
     def d_core(zz, side):
         at = zz if side == 0 else ep
-        return rcopy(dd.at[lines(zz, side, 1 - c), :], rc.at[at], rc_s.at[at], rc_r.at[at], pc)
+        return rcopy(dd.at[lines(zz, side, 1 - c), :], rc.at[at], sent.at[1], rc_r.at[at], pc)
 
     wide = width // HALVES
 
@@ -442,35 +444,37 @@
         return (
             rcopy(
                 dd.at[few(zz, c), part], back.at[zz, slots_of(c), part],
-                q_s.at[zz, h, 0], q_r.at[zz, h, 0], xn,
+                sent.at[1], q_r.at[zz, h], xn,
             ),
             rcopy(
                 dd.at[few(zz, 1 - c), part], back.at[zz, slots_of(c), part],
-                q_s.at[zz, h, 1], q_r.at[zz, h, 1], xd,
+                sent.at[1], q_r.at[zz, h], xd,
             ),
         )
 
     def d_x(p):
-        return rcopy(dd.at[lines(z, 1, c), cols(p)], rx.at[:, cols(p)], rx_s.at[p], rx_r.at[p], xn)
+        return rcopy(dd.at[lines(z, 1, c), cols(p)], rx.at[:, cols(p)], sent.at[2], rx_r.at[p], xn)
 
     def to_inner(zz, p):
         src = dd.at[lines(zz, 0, c), cols(p)]
-        return rcopy(src, edge_in.at[zz, :, cols(p)], e_s.at[zz, p], e_r.at[zz, p], (g, inner, t))
+        return rcopy(src, edge_in.at[zz, :, cols(p)], sent.at[2], e_r.at[zz, p], (g, inner, t))
 
     def to_owner(zz, p):
         owner_is_edge = jnp.logical_or(zz == 0, zz == ep - 1)
         place = jnp.where(jnp.logical_and(owner_is_edge, zz == outer), 0, 1)
         src = dd.at[lines(zz, 0, c), cols(p)]
-        return rcopy(src, last_in.at[place, :, cols(p)], f_s.at[zz, p], f_r.at[place, p], (g, zz, t))
+        return rcopy(src, last_in.at[place, :, cols(p)], sent.at[2], f_r.at[place, p], (g, zz, t))
 
     def last_arrival(place, p):
         here = last_in.at[place, :, cols(p)]
-        return rcopy(here, here, f_s.at[place, p], f_r.at[place, p], xn)
+        return rcopy(here, here, sent.at[2], f_r.at[place, p], xn)
 
     def compute(zz):
         core_step(zz, 1)
         experts(zz, 1)
         d_core(zz, 0).start()
+
+    def few_send(zz):
         for h in range(HALVES):
             for copy in d_few(zz, h):
                 copy.start()
@@ -488,8 +492,8 @@
         for p in range(PARTS):
             band = cols(p)
             if p % (PARTS // HALVES) == 0:
-                for copy in d_few(zz, p // (PARTS // HALVES)):
-                    copy.wait_recv()
+                h = p // (PARTS // HALVES)
+                arrived(back.at[zz, pl.ds(0, 2 * cap), pl.ds(h * wide, wide)], q_r.at[zz, h])
             so_far = (
                 dd[here, band].astype(F32)
                 + rc[zz, :, band].astype(F32)
@@ -520,11 +524,10 @@
 
     def m_x(h):
         part = pl.ds(h * wide, wide)
-        return rcopy(mp.at[(1 - x) * 2 + c, :, part], mrx.at[:, part], m_s.at[2 + h], m_r.at[2 + h], xn)
+        return rcopy(mp.at[(1 - x) * 2 + c, :, part], mrx.at[:, part], sent.at[2], m_r.at[1 + h], xn)
 
     def mixer_fold():
-        for xx in range(2):
-            m_core(xx).wait_recv()
+        arrived(mrc, m_r.at[0])
         mine = (1 - x) * 2 + c
         mp[mine] = (mp[mine].astype(F32) + mrc[1 - x].astype(F32)).astype(BF)
 
@@ -532,31 +535,33 @@
         m_x(h).start()
 
     z_step(1)
+    own_x()
     compacts(1)
-    own_x()
-    mixer()
     z_step(2)
     compacts(2)
+    mixer()
     for name in ("eg", "eu", "ed"):
         loads[name].wait()
     compute(order[1])
+    few_send(order[1])
     z_step(3)
     compacts(3)
+    compute(order[2])
     core_step(z, 2)
     shared()
     experts(z, 2)
     for side in range(2):
         d_core(z, side).start()
-    compute(order[2])
+    few_send(order[2])
     compute(order[3])
+    few_send(order[3])
     mixer_fold()
     mixer_send(0)
-    fold_z(target(1))
     mixer_send(1)
     fold_core()
+    fold_z(target(1))
     fold_z(target(2))
     fold_z(target(3))
-
     for h in range(HALVES):
         m_x(h).wait_recv()
     mixed = mp[t].astype(F32) + mrc[x].astype(F32) + mrx[...].astype(F32)
@@ -583,56 +588,38 @@
             to_inner(z, p).wait_recv()
             rows_ref[:, band] = (total + edge_in[z, :, band].astype(F32)).astype(BF)
 
-    @pl.when(has_up)
-    def _():
-        h_gate.wait_send()
-        h_value.wait_send()
-
-    for k in PIECES:
-        c_x(k).wait_send()
-    for p in range(PARTS):
-        d_x(p).wait_send()
-    for copy in core_pair(z, 1, c):
-        copy.wait_send()
-    d_core(z, 1).wait_send()
-
-    for zz in range(ep):
-        @pl.when(jnp.logical_and(has_up, zz <= z))
-        def _():
-            for k in PIECES:
-                c_up(zz, k).wait_send()
-
-        @pl.when(jnp.logical_and(has_down, zz >= z))
-        def _():
-            for k in PIECES:
-                c_down(zz, k).wait_send()
-
-        for copy in core_pair(zz, 0, c):
-            copy.wait_send()
-        d_core(zz, 0).wait_send()
-
-        @pl.when(zz != z)
-        def _():
-            for copy in few_pair(zz):
-                copy.wait_send()
-            for h in range(HALVES):
-                for copy in d_few(zz, h):
-                    copy.wait_send()
-
-        @pl.when(jnp.logical_and(zz != z, is_edge))
-        def _():
-            for p in range(PARTS):
-                to_inner(zz, p).wait_send()
-
-        @pl.when(jnp.logical_and(zz != z, jnp.logical_not(is_edge)))
-        def _():
-            for p in range(PARTS):
-                to_owner(zz, p).wait_send()
-
-    for xx in range(2):
-        m_core(xx).wait_send()
-    for h in range(HALVES):
-        m_x(h).wait_send()
+    def left(ref, sem):
+        rcopy(ref, ref, sem, m_r.at[0], xn).wait_send()
+
+    def drain():
+        @pl.when(has_up)
+        def _():
+            left(halo, sent.at[3])
+
+        for edge_chip, moved in ((True, 1), (False, 2 * ep - 3)):
+            total_blocks = moved + ep + 2
+
+            @pl.when(is_edge == edge_chip)
+            def _():
+                left(gat.at[pl.ds(0, total_blocks * rows), :], sent.at[0])
+                left(tab.at[pl.ds(0, total_blocks)], sent.at[0])
+
+        slots = 2 * (ep - 1) * 2 * cap
+        left(gat.at[pl.ds(0, slots + (ep + 1) * rows), :], sent.at[1])
+        left(gat.at[pl.ds(0, (1 + ep - 1 + 3) * rows), :], sent.at[2])
+
+    drain()
+
+
+def store_rows(mixed_ref, rows_ref, mixed_out, rows_out, sem):
+    copies = [
+        pltpu.make_async_copy(mixed_ref, mixed_out, sem.at[0]),
+        pltpu.make_async_copy(rows_ref, rows_out, sem.at[1]),
+    ]
+    for copy in copies:
+        copy.start()
+    for copy in copies:
+        copy.wait()
 
 
 def fused_on_device(ep, tp, *args):
@@ -650,7 +637,7 @@
     vmem = pl.BlockSpec(memory_space=pltpu.VMEM)
     dma = pltpu.SemaphoreType.DMA
     V = pltpu.VMEM
-    return pl.pallas_call(
+    mixed, summed = pl.pallas_call(
         functools.partial(fused_kernel, ep, tp, cap, slot),
         out_shape=(V((rows, width), BF), V((rows, width), BF)),
         in_specs=[any_spec] * 3 + [vmem, any_spec, vmem, any_spec, vmem, vmem, vmem] + [any_spec] * 6,
@@ -667,20 +654,26 @@
             V((ep + 1, rows, width), BF), V((ep, 2 * slot, width), BF), V((rows, width), BF),
             V((ep, rows, width), BF), V((2, rows, width), BF),
             V((tp, rows, width), BF), V((2, rows, width), BF), V((rows, width), BF),
-            dma((11,)), dma((4,)),
-            dma((ep, CHUNKS + 1)), dma((ep, CHUNKS + 1)), dma((ep, CHUNKS + 1)),
-            dma((CHUNKS + 1,)), dma((CHUNKS + 1,)), dma((ep, 2, 2)), dma((ep, 2, 2)),
-            dma((ep, 2)), dma((ep, 2)),
-            dma((ep + 1,)), dma((ep + 1,)), dma((ep, HALVES, 2)), dma((ep, HALVES, 2)),
-            dma((PARTS,)), dma((PARTS,)),
-            dma((ep, PARTS)), dma((ep, PARTS)), dma((2, PARTS)), dma((ep, PARTS)),
-            dma((2 + HALVES,)), dma((2 + HALVES,)),
+            dma((11,)), dma((2,)), dma((ep, CHUNKS + 1)), dma((CHUNKS + 1,)), dma((ep + 1, 2)), dma((ep,)),
+            dma((ep + 1,)), dma((ep, HALVES)), dma((PARTS,)), dma((ep, PARTS)), dma((2, PARTS)),
+            dma((1 + HALVES,)), dma((4,)),
         ],
         compiler_params=pltpu.CompilerParams(
             collective_id=0, has_side_effects=True, vmem_limit_bytes=60 * 1024 * 1024
         ),
     )(
         og, ig, iv, taps, mo, mgain.reshape(1, -1), tok, egain.reshape(1, -1), ids.T, wts.T, eg, eu, ed, sg, su, sd
+    )
+    out = jax.ShapeDtypeStruct((rows, width), BF)
+    return pl.pallas_call(
+        store_rows,
+        out_shape=(out, out),
+        in_specs=[vmem, vmem],
+        out_specs=(any_spec, any_spec),
+        scratch_shapes=[dma((2,))],
+    )(
+        pltpu.with_memory_space_constraint(mixed, pltpu.VMEM),
+        pltpu.with_memory_space_constraint(summed, pltpu.VMEM),
     )
 
 

time: 58.5 us -> 55.4 us (0.947)
  Pallas kernels: 56.1 us -> 54.6 us
  local copies, waits for them, and re-layouts: 1.41 us -> 0 us
    pallas_call x1, Pallas kernels: 56.1 us -> 53.7 us  [fused_on_device(): pl.pallas_call(functools.partial(fused_kernel, ep, tp, cap, slot), out_sh...]
    unnamed x2 -> x0, local copies, waits for them, and re-layouts: 1.41 us -> none
    pallas_call x0 -> x1, Pallas kernels: none -> 0.81 us  [fused_on_device(): pl.pallas_call(store_rows, out_shape=(out, out), in_specs=[vmem, vmem], o...]
where the time goes in v3:
time: 55.4 us; the launch traced here: 55.2 us
  Pallas kernels  54.6 us (99%)
  between operations  0.64 us (1%)
    pallas_call x1, Pallas kernels, fused_on_device(): pl.pallas_call(functools.partial(fused_kernel, ep, tp, cap, slot), out_sh...  53.7 us

profile of v3, /device:TPU:0, one launch (start us, length us, event | category | flops | bytes accessed | tf_op | source)
XLA Modules:
  0.0 55.2 jit_solution(10882611429142998309)
XLA Ops:
  0.6 53.7 %shard_map.167 = (bf16[64,2048]{1,0:T(8,128)(2,1)S(1)}, bf16[64,2048]{1,0:T(8,128)(2,1)S(1)}) custom-call(bf16[256,512]{1,0:T(8,128)(2,1)} %og_h.1, bf16[256,512]{1,0:T(8,128)(2,1)} %ig_h.1, bf16[256,512]{1,0:T(8,128)(2,1)} %iv_h.1, bf16[3,2048]{1,0:T(4,128)(2,1)} %taps.1, bf16[512,2048]{1,0:T(8,128)(2,1)} %mo_h.1, f32[1,2048]{1,0:T(1,128)} %bitcast.4, ...), custom_call_target="tpu_custom_call" | custom-call | tf_op jit(solution)/shard_map/pallas_call | solution.py:640
  54.4 0.8 %shard_map.168 = (bf16[64,2048]{1,0:T(8,128)(2,1)}, bf16[64,2048]{1,0:T(8,128)(2,1)}) custom-call(bf16[64,2048]{1,0:T(8,128)(2,1)S(1)} %get-tuple-element.4.mixed_ref, bf16[64,2048]{1,0:T(8,128)(2,1)S(1)} %get-tuple-element.5.rows_ref), custom_call_target="tpu_custom_call" | custom-call | tf_op jit(solution)/shard_map/pallas_call | solution.py:668

commit v4 on v3

--- a/solution.py
+++ b/solution.py
@@ -122,9 +122,9 @@
 
 def fused_kernel(
     ep, tp, cap, slot,
-    og_h, ig_h, iv_h, taps, mo_h, mgain, tok_h, egain, ids, wts, eg_h, eu_h, ed_h, sg_h, su_h, sd_h,
+    og_h, ig_h, iv_h, taps_h, mo_h, mgain_h, tok_h, egain_h, ids_h, wts_h, eg_h, eu_h, ed_h, sg_h, su_h, sd_h,
     mixed_ref, rows_ref,
-    og, ig, iv, mo, tok, eg, eu, ed, sgu, halo, pbuf, scaled,
+    og, ig, iv, mo, tok, taps, mgain, egain, ids, wts, eg, eu, ed, sgu, halo, pbuf, scaled,
     gat, tab, act, dd, packed, spread, rc, back, rx, edge_in, last_in, mp, mrc, mrx,
     load_sem, halo_sem, gz_r, gx_r, gc_r, px_r, rc_r, q_r, rx_r, e_r, f_r, m_r, sent,
 ):
@@ -159,8 +159,12 @@
     half = sd_h.shape[0]
     hid = eg.shape[1]
     load("tok", tok_h, tok)
+    load("egain", egain_h, egain)
+    load("ids", ids_h, ids)
+    load("wts", wts_h, wts)
     load("ig", ig_h, ig)
     load("iv", iv_h, iv)
+    load("taps", taps_h, taps)
     load("og", og_h, og)
     load("mo", mo_h, mo)
     load("sg", sg_h, sgu.at[:, pl.ds(0, half)])
@@ -169,6 +173,7 @@
     load("eg", eg_h.at[0], eg)
     load("eu", eu_h.at[0], eu)
     load("ed", ed_h.at[0], ed.at[pl.ds(0, hid), :])
+    load("mgain", mgain_h, mgain)
 
     barrier = pltpu.get_barrier_semaphore()
     for peer in (xn, pc, xd, z2):
@@ -239,7 +244,8 @@
         for e in range(2):
             back[zz, pl.ds(e * slot + cap, slot - cap), :] = jnp.zeros((slot - cap, width), BF)
 
-    loads["tok"].wait()
+    for name in ("tok", "egain", "ids", "wts"):
+        loads[name].wait()
     name_i = lax.broadcasted_iota(jnp.int32, (tab.shape[1], rows), 0)
     table = jnp.zeros((tab.shape[1], rows), F32)
     for k in range(ids.shape[0]):
@@ -299,6 +305,7 @@
             pbuf[:8, :] = halo[0, edge - 8 :, :].astype(F32) * halo[1, edge - 8 :, :].astype(F32)
 
         loads["og"].wait()
+        loads["taps"].wait()
         tap = taps[:, pl.ds(pl.multiple_of(t * columns, columns), columns)].astype(F32)
         filtered = (
             tap[0:1] * pbuf[6 : 6 + count, :] + tap[1:2] * pbuf[7 : 7 + count, :] + tap[2:3] * pbuf[8 : 8 + count, :]
@@ -564,6 +571,7 @@
     fold_z(target(3))
     for h in range(HALVES):
         m_x(h).wait_recv()
+    loads["mgain"].wait()
     mixed = mp[t].astype(F32) + mrc[x].astype(F32) + mrx[...].astype(F32)
     scale = lax.rsqrt(jnp.mean(mixed * mixed, axis=-1, keepdims=True) + EPSILON)
     mixed_ref[...] = (mixed * scale * mgain[...]).astype(BF)
@@ -640,11 +648,13 @@
     mixed, summed = pl.pallas_call(
         functools.partial(fused_kernel, ep, tp, cap, slot),
         out_shape=(V((rows, width), BF), V((rows, width), BF)),
-        in_specs=[any_spec] * 3 + [vmem, any_spec, vmem, any_spec, vmem, vmem, vmem] + [any_spec] * 6,
+        in_specs=[any_spec] * 16,
         out_specs=(vmem, vmem),
         scratch_shapes=[
             V((count, columns), BF), V((count, columns), BF), V((count, columns), BF),
             V((columns, width), BF), V((rows, width), BF),
+            V(taps.shape, BF), V((1, width), F32), V((1, width), F32),
+            V(ids.shape[::-1], jnp.int32), V(wts.shape[::-1], F32),
             V((width, hid), BF), V((width, hid), BF), V((hid + half, width), BF),
             V((width, 2 * half), BF),
             V((2, 16, columns), BF), V((count + 8, columns), F32), V((count, columns), BF),
@@ -654,7 +664,7 @@
             V((ep + 1, rows, width), BF), V((ep, 2 * slot, width), BF), V((rows, width), BF),
             V((ep, rows, width), BF), V((2, rows, width), BF),
             V((tp, rows, width), BF), V((2, rows, width), BF), V((rows, width), BF),
-            dma((11,)), dma((2,)), dma((ep, CHUNKS + 1)), dma((CHUNKS + 1,)), dma((ep + 1, 2)), dma((ep,)),
+            dma((16,)), dma((2,)), dma((ep, CHUNKS + 1)), dma((CHUNKS + 1,)), dma((ep + 1, 2)), dma((ep,)),
             dma((ep + 1,)), dma((ep, HALVES)), dma((PARTS,)), dma((ep, PARTS)), dma((2, PARTS)),
             dma((1 + HALVES,)), dma((4,)),
         ],

time: 55.4 us -> 54.7 us (0.987)
  Pallas kernels: 54.6 us -> 53.9 us
    pallas_call x1, Pallas kernels: 53.7 us -> 53.1 us  [fused_on_device(): pl.pallas_call(functools.partial(fused_kernel, ep, tp, cap, slot), out_sh...]
where the time goes in v4:
time: 54.7 us; the launch traced here: 54.6 us
  Pallas kernels  53.9 us (99%)
  between operations  0.64 us (1%)
    pallas_call x1, Pallas kernels, fused_on_device(): pl.pallas_call(functools.partial(fused_kernel, ep, tp, cap, slot), out_sh...  53.1 us

profile of v4, /device:TPU:0, one launch (start us, length us, event | category | flops | bytes accessed | tf_op | source)
XLA Modules:
  0.0 54.6 jit_solution(14801288817895228846)
XLA Ops:
  0.6 53.1 %shard_map.167 = (bf16[64,2048]{1,0:T(8,128)(2,1)S(1)}, bf16[64,2048]{1,0:T(8,128)(2,1)S(1)}) custom-call(bf16[256,512]{1,0:T(8,128)(2,1)} %og_h.1, bf16[256,512]{1,0:T(8,128)(2,1)} %ig_h.1, bf16[256,512]{1,0:T(8,128)(2,1)} %iv_h.1, bf16[3,2048]{1,0:T(4,128)(2,1)} %taps_h.1, bf16[512,2048]{1,0:T(8,128)(2,1)} %mo_h.1, f32[1,2048]{1,0:T(1,128)} %bitcast.4, ...), custom_call_target="tpu_custom_call" | custom-call | tf_op jit(solution)/shard_map/pallas_call | solution.py:648
  53.8 0.8 %shard_map.168 = (bf16[64,2048]{1,0:T(8,128)(2,1)}, bf16[64,2048]{1,0:T(8,128)(2,1)}) custom-call(bf16[64,2048]{1,0:T(8,128)(2,1)S(1)} %get-tuple-element.4.mixed_ref, bf16[64,2048]{1,0:T(8,128)(2,1)S(1)} %get-tuple-element.5.rows_ref), custom_call_target="tpu_custom_call" | custom-call | tf_op jit(solution)/shard_map/pallas_call | solution.py:678

commit v5 on v4

--- a/solution.py
+++ b/solution.py
@@ -149,6 +149,18 @@
     has_up = z < ep - 1
     has_down = z > 0
 
+    barrier = pltpu.get_barrier_semaphore()
+    for peer in (xn, pc, xd, z2):
+        pl.semaphore_signal(barrier, inc=1, device_id=peer, device_id_type=MESH)
+
+    @pl.when(has_up)
+    def _():
+        pl.semaphore_signal(barrier, inc=1, device_id=up, device_id_type=MESH)
+
+    @pl.when(has_down)
+    def _():
+        pl.semaphore_signal(barrier, inc=1, device_id=down, device_id_type=MESH)
+
     loads = {}
 
     def load(name, src, dst):
@@ -175,18 +187,6 @@
     load("ed", ed_h.at[0], ed.at[pl.ds(0, hid), :])
     load("mgain", mgain_h, mgain)
 
-    barrier = pltpu.get_barrier_semaphore()
-    for peer in (xn, pc, xd, z2):
-        pl.semaphore_signal(barrier, inc=1, device_id=peer, device_id_type=MESH)
-
-    @pl.when(has_up)
-    def _():
-        pl.semaphore_signal(barrier, inc=1, device_id=up, device_id_type=MESH)
-
-    @pl.when(has_down)
-    def _():
-        pl.semaphore_signal(barrier, inc=1, device_id=down, device_id_type=MESH)
-
     def rcopy(src, dst, ssem, rsem, peer):
         return pltpu.make_async_remote_copy(
             src_ref=src, dst_ref=dst, send_sem=ssem, recv_sem=rsem, device_id=peer, device_id_type=MESH
@@ -239,10 +239,6 @@
             rcopy(packed.at[zz, slots_of(c), :], gat.at[few(zz, c), :], sent.at[1], px_r.at[zz], xn),
             rcopy(packed.at[zz, slots_of(1 - c), :], gat.at[few(zz, c), :], sent.at[1], px_r.at[zz], xd),
         )
-
-    for zz in range(ep):
-        for e in range(2):
-            back[zz, pl.ds(e * slot + cap, slot - cap), :] = jnp.zeros((slot - cap, width), BF)
 
     for name in ("tok", "egain", "ids", "wts"):
         loads[name].wait()
@@ -281,6 +277,10 @@
 
         c_x(k).start()
     core_start(z, 0)
+
+    for zz in range(ep):
+        for e in range(2):
+            back[zz, pl.ds(e * slot + cap, slot - cap), :] = jnp.zeros((slot - cap, width), BF)
 
     count = ig.shape[0]
     tile = width // PARTS

time: 54.7 us -> 54.7 us (level)
  no operation moved by 1% of the time
where the time goes in v5:
time: 54.7 us; the launch traced here: 54.6 us
  Pallas kernels  53.9 us (99%)
  between operations  0.64 us (1%)
    pallas_call x1, Pallas kernels, fused_on_device(): pl.pallas_call(functools.partial(fused_kernel, ep, tp, cap, slot), out_sh...  53.1 us

profile of v5, /device:TPU:0, one launch (start us, length us, event | category | flops | bytes accessed | tf_op | source)
XLA Modules:
  0.0 54.6 jit_solution(15042255610918632931)
XLA Ops:
  0.6 53.1 %shard_map.167 = (bf16[64,2048]{1,0:T(8,128)(2,1)S(1)}, bf16[64,2048]{1,0:T(8,128)(2,1)S(1)}) custom-call(bf16[256,512]{1,0:T(8,128)(2,1)} %og_h.1, bf16[256,512]{1,0:T(8,128)(2,1)} %ig_h.1, bf16[256,512]{1,0:T(8,128)(2,1)} %iv_h.1, bf16[3,2048]{1,0:T(4,128)(2,1)} %taps_h.1, bf16[512,2048]{1,0:T(8,128)(2,1)} %mo_h.1, f32[1,2048]{1,0:T(1,128)} %bitcast.4, ...), custom_call_target="tpu_custom_call" | custom-call | tf_op jit(solution)/shard_map/pallas_call | solution.py:648
  53.8 0.8 %shard_map.168 = (bf16[64,2048]{1,0:T(8,128)(2,1)}, bf16[64,2048]{1,0:T(8,128)(2,1)}) custom-call(bf16[64,2048]{1,0:T(8,128)(2,1)S(1)} %get-tuple-element.4.mixed_ref, bf16[64,2048]{1,0:T(8,128)(2,1)S(1)} %get-tuple-element.5.rows_ref), custom_call_target="tpu_custom_call" | custom-call | tf_op jit(solution)/shard_map/pallas_call | solution.py:678
